TPU v7x, 32 devices: a whole 2x2x4 slice. The times are simulated.
32 devices in a mesh: sp: 8 (over z, core), tp: 4 (over y, x).
Axes of the slice: x: 2, y: 2, z: 4, core: 2. Of those that a mesh axis runs over, the one named last changes fastest.
Arguments:
- residual: bfloat16 [1024, 4096], P('sp', 'tp'), may hold values from -46 to 46
- query_small: bfloat16 [1024, 2048], P('sp', 'tp'), may hold values from -6 to 6
- key_narrow_group: bfloat16 [1024, 2048], P('sp', 'tp'), may hold values from -6 to 6
- query_large: bfloat16 [1024, 4096], P('sp', 'tp'), may hold values from -6 to 6
- key_large: bfloat16 [1024, 4096], P('sp', 'tp'), may hold values from -6 to 6
- values: bfloat16 [1024, 2, 2048], P('sp', None, 'tp'), may hold values from -6 to 6
- gates: bfloat16 [1024, 2, 2048], P('sp', None, 'tp'), may hold values from -6 to 6
- log_decay: float32 [1024, 2, 16], P('sp', None, 'tp'), may hold values from -0.65 to 0, as said below
- head_gain: float32 [2, 2048], P(None, 'tp'), may hold values from 0.1 to 1.9
- out_weight: bfloat16 [2, 2048, 4096], P(None, 'sp', 'tp'), may hold values from -0.09375 to 0.09375
- norm_gain: float32 [4096], P('tp'), may hold values from 0.1 to 1.9
- routes: int32 [1024, 2], P('sp'), may hold values from 0 to 7, all different within a row; in each aligned block of 128 rows (0 to 127, 128 to 255, ...) at most 64 rows name the same one
- route_weight: float32 [1024, 2], P('sp'), may hold values from 0.2 to 1
- expert_gate: bfloat16 [8, 4096, 2048], P('sp', None, 'tp'), may hold values from -0.09375 to 0.09375
- expert_up: bfloat16 [8, 4096, 2048], P('sp', None, 'tp'), may hold values from -0.09375 to 0.09375
- expert_down: bfloat16 [8, 2048, 4096], P('sp', None, 'tp'), may hold values from -0.5 to 0.5
Outputs:
- new_stream: bfloat16 [1024, 4096], P('sp', 'tp')
Inputs may be any that keep to these rules, and one draw needn't show every extreme that they name: `routes`: each row names two different experts; in each aligned block of 128 rows no expert is named more than 64 times, a bound that some block reaches. `log_decay`: negative at every position.
All inputs are finite; a program needn't handle non-finite values.
Results may differ from a plain program's by a relative error of at most 0.019.
Values may be sent and summed in bfloat16 or wider, within the bound.
A program may use at most 64 MiB of HBM per device.

v0:
```python
import jax
import jax.numpy as jnp
from jax import lax
from jax.experimental import pallas as pl
from jax.experimental.pallas import tpu as pltpu
from jax.sharding import PartitionSpec as P

MESH = pl.DeviceIdType.MESH


EPS = 1e-06
THETA = 10000.0


def greet(axes):
    barrier = pltpu.get_barrier_semaphore()
    total = 0
    for axis in axes:
        count, me = lax.axis_size(axis), lax.axis_index(axis)

        def signal(k, _, axis=axis, count=count, me=me):
            pl.semaphore_signal(
                barrier, inc=1, device_id={axis: (me + k) % count}, device_id_type=MESH
            )
            return 0

        lax.fori_loop(1, count, signal, 0)
        total += count - 1
    pl.semaphore_wait(barrier, total)


def remote(source, target, send_sem, recv_sem, axis, index):
    return pltpu.make_async_remote_copy(
        src_ref=source,
        dst_ref=target,
        send_sem=send_sem,
        recv_sem=recv_sem,
        device_id={axis: index},
        device_id_type=MESH,
    )


def chain_kernel(update_ref, fall_ref, out_ref, held, outgoing, send_sem, recv_sem):
    count, me = lax.axis_size("sp"), lax.axis_index("sp")
    pieces = update_ref.shape[0]
    right, left = (me + 1) % count, (me + count - 1) % count
    barrier = pltpu.get_barrier_semaphore()
    for neighbour in (left, right):
        pl.semaphore_signal(barrier, inc=1, device_id={"sp": neighbour}, device_id_type=MESH)
    pl.semaphore_wait(barrier, 2)

    def hop(c):
        return remote(
            outgoing.at[c], held.at[c], send_sem.at[c], recv_sem.at[c], "sp", right
        )

    def step(c, _):
        @pl.when(me == 0)
        def _():
            held[c] = jnp.zeros(held.shape[1:], held.dtype)

        @pl.when(me > 0)
        def _():
            hop(c).wait_recv()

        @pl.when(me < count - 1)
        def _():
            outgoing[c] = (fall_ref[c] * held[c].astype(jnp.float32) + update_ref[c]).astype(
                outgoing.dtype
            )
            hop(c).start()

        out_ref[c] = held[c]
        return 0

    lax.fori_loop(0, pieces, step, 0)

    @pl.when(me < count - 1)
    def _():
        def finish(c, _):
            hop(c).wait_send()
            return 0

        lax.fori_loop(0, pieces, finish, 0)


def entering_states(update, fall):
    pieces, rows, columns = update.shape
    return pl.pallas_call(
        chain_kernel,
        out_shape=jax.ShapeDtypeStruct(update.shape, jnp.bfloat16),
        in_specs=[pl.BlockSpec(memory_space=pltpu.VMEM)] * 2,
        out_specs=pl.BlockSpec(memory_space=pltpu.VMEM),
        scratch_shapes=[
            pltpu.VMEM((pieces, rows, columns), jnp.bfloat16),
            pltpu.VMEM((pieces, rows, columns), jnp.bfloat16),
            pltpu.SemaphoreType.DMA((pieces,)),
            pltpu.SemaphoreType.DMA((pieces,)),
        ],
        compiler_params=pltpu.CompilerParams(collective_id=0, has_side_effects=True),
    )(update, fall)


def gather_kernel(part_ref, out_ref, held, send_sem, recv_sem):
    count, me = lax.axis_size("tp"), lax.axis_index("tp")
    width = part_ref.shape[2]
    greet(("tp",))

    def place(index):
        return held.at[:, :, pl.ds(pl.multiple_of(index * width, width), width)]

    def start(k, _):
        remote(part_ref, place(me), send_sem.at[k], recv_sem.at[me], "tp", (me + k) % count).start()
        return 0

    lax.fori_loop(1, count, start, 0)
    held[:, :, pl.ds(pl.multiple_of(me * width, width), width)] = part_ref[...]

    def finish(k, _):
        other = (me + k) % count
        remote(part_ref, place(other), send_sem.at[k], recv_sem.at[other], "tp", other).wait()
        return 0

    lax.fori_loop(1, count, finish, 0)
    out_ref[...] = held[...]


def gather_heads(part, count):
    whole = part.shape[:2] + (part.shape[2] * count,)
    return pl.pallas_call(
        gather_kernel,
        out_shape=jax.ShapeDtypeStruct(whole, part.dtype),
        in_specs=[pl.BlockSpec(memory_space=pltpu.VMEM)],
        out_specs=pl.BlockSpec(memory_space=pltpu.VMEM),
        scratch_shapes=[
            pltpu.VMEM(whole, part.dtype),
            pltpu.SemaphoreType.DMA((count,)),
            pltpu.SemaphoreType.DMA((count,)),
        ],
        compiler_params=pltpu.CompilerParams(collective_id=1, has_side_effects=True),
    )(part)


def experts_kernel(
    stream_ref,
    gain_ref,
    select_ref,
    gate_hbm,
    up_hbm,
    down_hbm,
    out_ref,
    w_gate,
    w_up,
    w_down,
    squares,
    outgoing,
    arrived,
    hidden,
    result,
    returned,
    acc_a,
    acc_b,
    acc_c,
    load_sem,
    sq_send,
    sq_recv,
    disp_send,
    disp_recv,
    fwd_send,
    fwd_recv,
    fwd_relay_send,
    fwd_relay_recv,
    hid_send,
    hid_recv,
    hid_relay_send,
    hid_relay_recv,
    ret_send,
    ret_recv,
):
    n_sp, n_tp = lax.axis_size("sp"), lax.axis_size("tp")
    s, t = lax.axis_index("sp"), lax.axis_index("tp")
    per_group = n_sp // GROUPS
    across, down = grid_of(n_tp)
    x, y = t % across, t // across
    cap = outgoing.shape[0] // n_sp
    cols = stream_ref.shape[1]
    units = w_gate.shape[1]
    loads = [
        pltpu.make_async_copy(source.at[0], target, load_sem.at[i])
        for i, (source, target) in enumerate(
            ((gate_hbm, w_gate), (up_hbm, w_up), (down_hbm, w_down))
        )
    ]
    for load in loads:
        load.start()
    greet(("sp", "tp"))

    def rows_of(p):
        return pl.ds(pl.multiple_of(p * cap, cap), cap)

    def group_base(g):
        return ((s // per_group + g) % GROUPS) * per_group

    def group_rows(g, part=None):
        size = per_group * cap
        start = pl.multiple_of(group_base(g) * cap, size)
        if part is None:
            return pl.ds(start, size)
        return pl.ds(pl.multiple_of(start + part * (size // 2), size // 2), size // 2)

    lines = (
        [y * across + (x + k) % across for k in range(1, across)],
        [((y + k) % down) * across + x for k in range(1, down)],
    )
    direct = lines[0] + lines[1]

    stream = stream_ref[...]
    own = jnp.sum(stream * stream, axis=1, keepdims=True)
    squares[t] = jnp.broadcast_to(own, squares.shape[1:])

    def square_copy(k, source):
        block, other = squares.at[source], (t + k) % n_tp
        return remote(block, block, sq_send.at[k], sq_recv.at[source], "tp", other)

    def square_start(k, _):
        square_copy(k, t).start()
        return 0

    def square_wait(k, _):
        square_copy(k, (t + k) % n_tp).wait()
        return 0

    lax.fori_loop(1, n_tp, square_start, 0)
    lax.fori_loop(1, n_tp, square_wait, 0)
    total = squares[0]
    for p in range(1, n_tp):
        total = total + squares[p]
    scale = lax.rsqrt(total[:, 0:1] / (cols * n_tp) + EPS)
    normed = (stream_ref[...] * scale * gain_ref[...]).astype(jnp.bfloat16)
    outgoing[...] = jnp.dot(
        select_ref[...], normed, preferred_element_type=jnp.float32
    ).astype(jnp.bfloat16)

    def dispatch(p, q):
        return remote(
            outgoing.at[rows_of(p)],
            arrived.at[t, rows_of(q)],
            disp_send.at[p],
            disp_recv.at[q],
            "sp",
            p,
        )

    def members(g, action):
        def body(j, _):
            action(group_base(g) + (s + j) % per_group)
            return 0

        lax.fori_loop(0, per_group, body, 0)

    def others(g, action):
        def guarded(p):
            @pl.when(p != s)
            def _():
                action(p)

        members(g, guarded)

    for g in range(GROUPS):
        others(g, lambda p: dispatch(p, s).start())
    arrived[t, rows_of(s)] = outgoing[rows_of(s)]

    def straight(buffer, sems, g, i, source, rows):
        block = buffer.at[source, rows]
        return remote(block, block, sems[0].at[g, i], sems[1].at[g, source], "tp", direct[i])

    def relayed(buffer, sems, g, part, i, source, target):
        block = buffer.at[source, group_rows(g, part)]
        return remote(
            block, block, sems[2].at[g, part, i], sems[3].at[g, source, part], "tp", target
        )

    def relay(buffer, sems, g):
        for part in range(2):
            for k, source in enumerate(lines[part]):
                i = k if part == 0 else len(lines[0]) + k
                straight(buffer, sems, g, i, source, group_rows(g)).wait_recv()
                for j, target in enumerate(lines[1 - part]):
                    relayed(
                        buffer, sems, g, part, k * len(lines[1 - part]) + j, source, target
                    ).start()

    def place_of(k):
        return ((y + k // across) % down) * across + (x + k % across) % across

    def wait_relayed(buffer, sems, g, k):
        @pl.when((k // across) * (k % across) > 0)
        def _():
            source = place_of(k)
            for part in range(2):
                relayed(buffer, sems, g, part, 0, source, source).wait_recv()

    def finish_sends(buffer, sems, g):
        for i in range(len(direct)):
            straight(buffer, sems, g, i, t, group_rows(g)).wait_send()
        for part in range(2):
            for i in range(len(lines[0]) * len(lines[1])):
                relayed(buffer, sems, g, part, i, t, direct[0]).wait_send()

    arrived_sems = (fwd_send, fwd_recv, fwd_relay_send, fwd_relay_recv)
    hidden_sems = (hid_send, hid_recv, hid_relay_send, hid_relay_recv)

    def forward(g):
        def block(p):
            @pl.when(p != s)
            def _():
                dispatch(p, p).wait_recv()

            for i in range(len(direct)):
                straight(arrived, arrived_sems, g, i, t, rows_of(p)).start()

        members(g, block)

    def through_units(g):
        acc_a[...] = jnp.zeros_like(acc_a)
        acc_b[...] = jnp.zeros_like(acc_b)

        def body(k, _):
            wait_relayed(arrived, arrived_sems, g, k)
            p = place_of(k)
            part = pl.ds(pl.multiple_of(p * cols, cols), cols)
            rows = arrived[p, group_rows(g)]
            acc_a[...] += jnp.dot(rows, w_gate[part, :], preferred_element_type=jnp.float32)
            acc_b[...] += jnp.dot(rows, w_up[part, :], preferred_element_type=jnp.float32)
            return 0

        lax.fori_loop(0, n_tp, body, 0)
        hidden[t, group_rows(g)] = (jax.nn.silu(acc_a[...]) * acc_b[...]).astype(jnp.bfloat16)
        for i in range(len(direct)):
            straight(hidden, hidden_sems, g, i, t, group_rows(g)).start()

    def give_back(p, q):
        return remote(
            result.at[rows_of(p)], returned.at[rows_of(q)], ret_send.at[p], ret_recv.at[q], "sp", p
        )

    def through_down(g):
        acc_c[...] = jnp.zeros_like(acc_c)

        def body(k, _):
            wait_relayed(hidden, hidden_sems, g, k)
            p = place_of(k)
            part = pl.ds(pl.multiple_of(p * units, units), units)
            acc_c[...] += jnp.dot(
                hidden[p, group_rows(g)], w_down[part, :], preferred_element_type=jnp.float32
            )
            return 0

        lax.fori_loop(0, n_tp, body, 0)
        result[group_rows(g)] = acc_c[...].astype(jnp.bfloat16)
        others(g, lambda p: give_back(p, s).start())

    for step in range(GROUPS + 4):
        for late, action in enumerate(
            (
                forward,
                lambda g: relay(arrived, arrived_sems, g),
                through_units,
                lambda g: relay(hidden, hidden_sems, g),
                through_down,
            )
        ):
            if 0 <= step - late < GROUPS:
                if late == 2 and step == 2:
                    for load in loads:
                        load.wait()
                action(step - late)
    returned[rows_of(s)] = result[rows_of(s)]
    for g in range(GROUPS):
        others(g, lambda p: give_back(p, p).wait_recv())
    out_ref[...] = returned[...]
    for g in range(GROUPS):
        others(g, lambda p: dispatch(p, s).wait_send())
        others(g, lambda p: give_back(p, s).wait_send())
        finish_sends(arrived, arrived_sems, g)
        finish_sends(hidden, hidden_sems, g)


GROUPS = 4


def grid_of(count):
    across = max(k for k in range(1, count + 1) if count % k == 0 and k * k <= count)
    return across, count // across


def through_experts(stream, gain, select, w_gate, w_up, w_down, n_sp, n_tp):
    count, cols = stream.shape
    slots = select.shape[0]
    width, units = w_gate.shape[1:]
    bf16, f32 = jnp.bfloat16, jnp.float32
    dma = pltpu.SemaphoreType.DMA
    across, down = grid_of(n_tp)
    straights, relays = across + down - 2, (across - 1) * (down - 1)
    vmem = pl.BlockSpec(memory_space=pltpu.VMEM)
    hbm = pl.BlockSpec(memory_space=pl.ANY)
    return pl.pallas_call(
        experts_kernel,
        out_shape=jax.ShapeDtypeStruct((slots, cols), bf16),
        in_specs=[vmem] * 3 + [hbm] * 3,
        out_specs=vmem,
        scratch_shapes=[
            pltpu.VMEM((width, units), bf16),
            pltpu.VMEM((width, units), bf16),
            pltpu.VMEM(w_down.shape[1:], bf16),
            pltpu.VMEM((n_tp, count, 128), f32),
            pltpu.VMEM((slots, cols), bf16),
            pltpu.VMEM((n_tp, slots, cols), bf16),
            pltpu.VMEM((n_tp, slots, units), bf16),
            pltpu.VMEM((slots, cols), bf16),
            pltpu.VMEM((slots, cols), bf16),
            pltpu.VMEM((slots // GROUPS, units), f32),
            pltpu.VMEM((slots // GROUPS, units), f32),
            pltpu.VMEM((slots // GROUPS, cols), f32),
            dma((3,)),
            dma((n_tp,)),
            dma((n_tp,)),
            dma((n_sp,)),
            dma((n_sp,)),
            dma((GROUPS, straights)),
            dma((GROUPS, n_tp)),
            dma((GROUPS, 2, relays)),
            dma((GROUPS, n_tp, 2)),
            dma((GROUPS, straights)),
            dma((GROUPS, n_tp)),
            dma((GROUPS, 2, relays)),
            dma((GROUPS, n_tp, 2)),
            dma((n_sp,)),
            dma((n_sp,)),
        ],
        compiler_params=pltpu.CompilerParams(
            collective_id=2, has_side_effects=True, vmem_limit_bytes=50 * 2**20
        ),
    )(stream, gain, select, w_gate, w_up, w_down)


def rotate(block, positions):
    half_dim = block.shape[-1] // 2
    inverse = jnp.power(THETA, -jnp.arange(half_dim, dtype=jnp.float32) * 2.0 / block.shape[-1])
    angles = positions[:, None, None] * inverse
    cosine_val, sine_val = (jnp.cos(angles), jnp.sin(angles))
    lower_half, upper_half = (block[..., :half_dim], block[..., half_dim:])
    return jnp.concatenate(
        [
            lower_half * cosine_val - upper_half * sine_val,
            upper_half * cosine_val + lower_half * sine_val,
        ],
        axis=-1,
    )


def block_terms(rot_queries, rot_keys, value_heads, rates):
    count = rates.shape[0]
    decay_sum = jnp.cumsum(rates, axis=0)
    by_head = decay_sum.T
    causal = (jnp.arange(count)[:, None] >= jnp.arange(count)[None, :])[None]
    spread = by_head[:, :, None] - by_head[:, None, :]
    weight = jnp.where(causal, jnp.exp(jnp.where(causal, spread, 0.0)), 0.0)
    scores = jnp.einsum("ihd,jhd->hij", rot_queries, rot_keys, preferred_element_type=jnp.float32)
    weighted = (scores * weight).astype(jnp.bfloat16)
    within = jnp.einsum("hij,jhv->ihv", weighted, value_heads, preferred_element_type=jnp.float32)
    block_end = decay_sum[-1]
    carried = (
        rot_keys.astype(jnp.float32) * jnp.exp(block_end[None, :] - decay_sum)[:, :, None]
    ).astype(jnp.bfloat16)
    update = jnp.einsum("jhd,jhv->hdv", carried, value_heads, preferred_element_type=jnp.float32)
    return (within, decay_sum, jnp.exp(block_end), update)


def final_result(rot_queries, decay_sum, within, state_in, gate_part, gain_part):
    cross_part = (
        jnp.einsum(
            "ihd,hdv->ihv",
            rot_queries,
            state_in,
            preferred_element_type=jnp.float32,
        )
        * jnp.exp(decay_sum)[:, :, None]
    )
    retained = within + cross_part
    scaled = retained * lax.rsqrt(jnp.mean(retained * retained, axis=-1, keepdims=True) + EPS)
    count, head_count, value_size = retained.shape
    gated = jax.nn.silu(gate_part.astype(jnp.float32)).reshape(count, head_count, value_size)
    return (
        (scaled * gain_part.reshape(head_count, value_size) * gated)
        .reshape(count, -1)
        .astype(jnp.bfloat16)
    )


def prepare(queries, keys_in, value_part, positions, head_count):
    row_count = queries.shape[0]
    key_size = queries.shape[1] // head_count
    rot_queries = rotate(
        queries.astype(jnp.float32).reshape(row_count, head_count, key_size), positions
    ).astype(jnp.bfloat16)
    rot_keys = (
        rotate(keys_in.astype(jnp.float32).reshape(row_count, head_count, key_size), positions)
        * key_size ** (-0.5)
    ).astype(jnp.bfloat16)
    value_heads = value_part.reshape(row_count, head_count, value_part.shape[1] // head_count)
    return (rot_queries, rot_keys, value_heads)


def per_device(
    residual,
    query_small,
    key_narrow_group,
    query_large,
    key_large,
    values,
    gates,
    log_decay,
    head_gain,
    out_weight,
    norm_gain,
    routes,
    route_weight,
    expert_gate,
    expert_up,
    expert_down,
):
    row_count = residual.shape[0]
    head_count = log_decay.shape[2]
    positions = (lax.axis_index("sp") * row_count + jnp.arange(row_count, dtype=jnp.int32)).astype(
        jnp.float32
    )
    query_a, key_a, value_a = prepare(
        query_small, key_narrow_group, values[:, 0], positions, head_count
    )
    query_b, key_b, value_b = prepare(query_large, key_large, values[:, 1], positions, head_count)
    within_a, decay_sum_a, fall_a, update_a = block_terms(query_a, key_a, value_a, log_decay[:, 0])
    within_b, decay_sum_b, fall_b, update_b = block_terms(query_b, key_b, value_b, log_decay[:, 1])

    n_sp, n_tp = lax.axis_size("sp"), lax.axis_size("tp")
    value_size = update_a.shape[2]
    piece = update_a.shape[1]
    parts = update_b.shape[1] // piece
    update = jnp.concatenate([update_a, update_b.reshape(-1, piece, value_size)], axis=0)
    fall = jnp.concatenate([fall_a, jnp.repeat(fall_b, parts)])
    fall = jnp.broadcast_to(fall[:, None, None], (fall.shape[0], 1, value_size))
    entering = entering_states(update, fall)
    state_a = entering[:head_count]
    state_b = entering[head_count:].reshape(update_b.shape)
    output_a = final_result(query_a, decay_sum_a, within_a, state_a, gates[:, 0], head_gain[0])
    output_b = final_result(query_b, decay_sum_b, within_b, state_b, gates[:, 1], head_gain[1])
    gathered = gather_heads(jnp.stack([output_a, output_b], axis=0), n_tp)
    weight = lax.all_gather(out_weight, "sp", axis=1, tiled=True)
    mixed = (
        jnp.dot(gathered[0], weight[0], preferred_element_type=jnp.float32)
        + jnp.dot(gathered[1], weight[1], preferred_element_type=jnp.float32)
    ).astype(jnp.bfloat16)
    stream = residual.astype(jnp.float32) + mixed.astype(jnp.float32)
    experts = lax.axis_size("sp")
    capacity = 4 * row_count // experts
    one_hot = (routes[:, :, None] == jnp.arange(experts, dtype=jnp.int32)[None, None, :]).astype(
        jnp.int32
    )
    one_hot = one_hot.reshape(2 * row_count, experts)
    before = jnp.cumsum(one_hot, axis=0) - one_hot
    slot_index = jnp.sum(before * one_hot, axis=1).reshape(row_count, 2)
    target = routes * capacity + slot_index
    slot_ids = jnp.arange(experts * capacity, dtype=jnp.int32)
    choose = target[:, :, None] == slot_ids[None, None, :]
    select = jnp.sum(choose.astype(jnp.int32), axis=1).astype(jnp.bfloat16).T
    returned = through_experts(
        stream, norm_gain[None, :], select, expert_gate, expert_up, expert_down, n_sp, n_tp
    )
    first_pick = jnp.dot(
        choose[:, 0].astype(jnp.bfloat16), returned, preferred_element_type=jnp.float32
    )
    second_pick = jnp.dot(
        choose[:, 1].astype(jnp.bfloat16), returned, preferred_element_type=jnp.float32
    )
    routed = route_weight[:, 0:1] * first_pick + route_weight[:, 1:2] * second_pick
    return (stream + routed).astype(jnp.bfloat16)


def solution(mesh):
    placed = (
        P("sp", "tp"),
        P("sp", "tp"),
        P("sp", "tp"),
        P("sp", "tp"),
        P("sp", "tp"),
        P("sp", None, "tp"),
        P("sp", None, "tp"),
        P("sp", None, "tp"),
        P(None, "tp"),
        P(None, "sp", "tp"),
        P("tp"),
        P("sp", None),
        P("sp", None),
        P("sp", None, "tp"),
        P("sp", None, "tp"),
        P("sp", None, "tp"),
    )
    return jax.shard_map(
        per_device, mesh=mesh, in_specs=placed, out_specs=P("sp", "tp"), check_vma=False
    )
```

profile of v0, /device:TPU:1, one launch (start us, length us, event | category | flops | bytes accessed | tf_op | source)
XLA Modules:
  0.0 200.9 jit_solution(6584012079770270556)
XLA Ops:
  6.5 0.7 all-gather.2.cloned.1.call-update
  7.3 0.8 copy.156
  8.3 1.1 copy.131
  9.8 1.1 copy.145
  11.6 0.7 fusion.70
  12.3 0.4 fusion.64
  12.7 0.2 copy.176
  14.1 0.2 copy.127
  14.5 0.6 copy.125
  15.2 0.4 fusion.63
  15.9 0.3 multiply_cosine_fusion.1
  16.5 0.3 multiply_cosine_fusion
  16.8 0.3 fusion.31
  17.1 0.8 multiply_subtract_fusion
  17.9 0.4 fusion.20
  18.3 1.0 pad_maximum_fusion.update_ref
  19.3 0.7 broadcast_in_dim.39.fall_ref
  20.0 20.7 %shard_map.154 = bf16[12,128,128]{2,1,0:T(8,128)(2,1)} custom-call(f32[12,128,128]{2,1,0:T(8,128)} %pad_maximum_fusion.update_ref, f32[12,1,128]{2,1,0:T(1,128)} %broadcast_in_dim.39.fall_ref), custom_call_target="tpu_custom_call" | custom-call | tf_op jit(solution)/shard_map/pallas_call | solution.py:89
  40.8 1.1 convolution_bitcast_fusion.3
  41.9 1.2 multiply_reduce_fusion.1
  43.8 0.4 convolution_bitcast_fusion.2
  44.2 0.3 multiply_reduce_fusion
  44.7 0.7 pad_maximum_fusion.2.part_ref
  45.5 11.6 %shard_map.155 = bf16[2,128,2048]{2,1,0:T(8,128)(2,1)} custom-call(bf16[2,128,512]{2,1,0:T(8,128)(2,1)} %pad_maximum_fusion.2.part_ref), custom_call_target="tpu_custom_call" | custom-call | tf_op jit(solution)/shard_map/pallas_call | solution.py:130
  57.1 0.6 reduce-window.6
  57.7 0.2 slice_reduce_fusion
  58.7 34.8 %all-gather.2.cloned.1.call-done = bf16[2,2048,1024]{2,1,0:T(8,128)(2,1)} async-done(((bf16[2,256,1024]{2,1,0:T(8,128)(2,1)}), bf16[2,2048,1024]{2,1,0:T(8,128)(2,1)}) %all-gather.2.cloned.1.call-update) | async-done | bytes 8388624 | tf_op jit(solution)/shard_map/all_gather | solution.py:558
  93.5 3.1 %fusion = f32[128,1024]{1,0:T(8,128)S(1)} fusion(bf16[2,2048,1024]{2,1,0:T(8,128)(2,1)} %all-gather.2.cloned.1.call-done, bf16[2,128,2048]{2,1,0:T(8,128)(2,1)} %shard_map.155), kind=kOutput, calls=%fused_computation.1 | convolution fusion | flops 536870912 | bytes 5242880 | tf_op jit(solution)/shard_map/dot_general | solution.py:561
  96.6 2.9 %fusion.7.stream_ref = f32[128,1024]{1,0:T(8,128)S(1)} fusion(f32[128,1024]{1,0:T(8,128)S(1)} %fusion, bf16[2,2048,1024]{2,1,0:T(8,128)(2,1)} %all-gather.2.cloned.1.call-done, bf16[2,128,2048]{2,1,0:T(8,128)(2,1)S(1)} %copy-done.1, bf16[128,1024]{1,0:T(8,128)(2,1)S(1)} %copy-done.12), kind=kOutput, calls=%fused_computation.11 | convolution fusion | flops 537526272 | bytes 6029312 | tf_op jit(solution)/shard_map/dot_general | solution.py:560
  99.6 93.2 %shard_map.156 = bf16[512,1024]{1,0:T(8,128)(2,1)S(1)} custom-call(f32[128,1024]{1,0:T(8,128)S(1)} %fusion.7.stream_ref, f32[1,1024]{1,0:T(1,128)S(1)} %bitcast.98, bf16[512,128]{1,0:T(8,128)(2,1)S(1)} %convert_bitcast_fusion.select_ref, bf16[1,4096,512]{2,1,0:T(8,128)(2,1)} %gate_hbm.1, bf16[1,4096,512]{2,1,0:T(8,128)(2,1)} %up_hbm.1, ...), custom_call_target="tpu_custom_call" | custom-call | tf_op jit(solution)/shard_map/pallas_call | solution.py:407
  192.7 0.3 convolution_multiply_fusion.1
  193.1 1.0 fusion.8
  (91 shorter events, 4.8 us)
Async XLA Ops:
  6.5 4.7 %copy-start.9 = (f32[128,2,4]{0,2,1:T(4,128)S(1)}, f32[128,2,4]{0,2,1:T(4,128)}, u32[]{:S(2)}) copy-start(f32[128,2,4]{0,2,1:T(4,128)} %param.23) | copy-start | bytes 12292
  6.5 5.8 %copy-start.2 = (bf16[128,2,512]{2,1,0:T(2,128)(2,1)S(1)}, bf16[128,2,512]{2,1,0:T(2,128)(2,1)}, u32[]{:S(2)}) copy-start(bf16[128,2,512]{2,1,0:T(2,128)(2,1)} %param.21) | copy-start | bytes 786436
  6.5 6.3 %copy-start.6 = (bf16[128,512]{1,0:T(8,128)(2,1)S(1)}, bf16[128,512]{1,0:T(8,128)(2,1)}, u32[]{:S(2)}) copy-start(bf16[128,512]{1,0:T(8,128)(2,1)} %param.17) | copy-start | bytes 393220
  6.5 87.0 %all-gather.2.cloned.1.call-start = ((), (), s32[]{:S(2)}) async-start(), calls=%async_computation | async-start | bytes 9437184 | tf_op jit(solution)/shard_map/all_gather | solution.py:558
  9.5 3.8 %copy-start.7 = (bf16[128,512]{1,0:T(8,128)(2,1)S(1)}, bf16[128,512]{1,0:T(8,128)(2,1)}, u32[]{:S(2)}) copy-start(bf16[128,512]{1,0:T(8,128)(2,1)} %param.18) | copy-start | bytes 393220
  10.9 4.3 %copy-start.3 = (bf16[128,2,512]{2,1,0:T(2,128)(2,1)S(1)}, bf16[128,2,512]{2,1,0:T(2,128)(2,1)}, u32[]{:S(2)}) copy-start(bf16[128,2,512]{2,1,0:T(2,128)(2,1)} %param.22) | copy-start | bytes 786436
  17.9 25.2 %copy-start.10 = (f32[2,512]{1,0:T(2,128)S(1)}, f32[2,512]{1,0:T(2,128)}, u32[]{:S(2)}) copy-start(f32[2,512]{1,0:T(2,128)} %param.24) | copy-start | bytes 12292
  17.9 25.6 %copy-start.5 = (f32[128,4]{1,0:T(8,128)S(1)}, f32[128,4]{1,0:T(8,128)}, u32[]{:S(2)}) copy-start(f32[128,4]{1,0:T(8,128)} %get-tuple-element.31) | copy-start | bytes 6148
  17.9 25.8 %copy-start.4 = (bf16[128,4,128]{2,0,1:T(8,128)(2,1)S(1)}, bf16[128,4,128]{2,0,1:T(8,128)(2,1)}, u32[]{:S(2)}) copy-start(bf16[128,4,128]{2,0,1:T(8,128)(2,1)} %get-tuple-element.28) | copy-start | bytes 393220
  40.7 3.4 %slice-start = ((bf16[12,128,128]{2,1,0:T(8,128)(2,1)}), bf16[8,128,128]{2,1,0:T(8,128)(2,1)S(1)}, s32[]{:S(2)}) async-start(bf16[12,128,128]{2,1,0:T(8,128)(2,1)} %shard_map.154), calls=%async_computation.1 | async-start | bytes 524288 | tf_op jit(solution)/shard_map/slice | solution.py:554
  41.9 16.3 %copy-start.8 = (s32[128,2]{0,1:T(2,128)S(1)}, s32[128,2]{0,1:T(2,128)}, u32[]{:S(2)}) copy-start(s32[128,2]{0,1:T(2,128)} %param.27) | copy-start | bytes 3076
  43.2 15.4 %copy-start.11 = (f32[128,2]{0,1:T(2,128)S(1)}, f32[128,2]{0,1:T(2,128)}, u32[]{:S(2)}) copy-start(f32[128,2]{0,1:T(2,128)} %param.28) | copy-start | bytes 3076
  57.1 39.5 %copy-start.1 = (bf16[2,128,2048]{2,1,0:T(8,128)(2,1)S(1)}, bf16[2,128,2048]{2,1,0:T(8,128)(2,1)}, u32[]{:S(2)}) copy-start(bf16[2,128,2048]{2,1,0:T(8,128)(2,1)} %shard_map.155) | copy-start | bytes 3145732
  57.1 39.5 %copy-start.12 = (bf16[128,1024]{1,0:T(8,128)(2,1)S(1)}, bf16[128,1024]{1,0:T(8,128)(2,1)}, u32[]{:S(2)}) copy-start(bf16[128,1024]{1,0:T(8,128)(2,1)} %param.16) | copy-start | bytes 786436
  96.6 3.0 %copy-start = (f32[1024]{0:T(1024)S(1)}, f32[1024]{0:T(1024)}, u32[]{:S(2)}) copy-start(f32[1024]{0:T(1024)} %param.26) | copy-start | bytes 12292
Sparse Core Ops, SparseCore 0:
  8.9 84.5 all-gather.1
where the time goes:
time: 202 us; the launch traced here: 201 us
  Pallas kernels  125 us (62%)
  waiting for transfers between devices  35.5 us (18%)
  between operations  14 us (7%)
  matrix products  11.1 us (5%)
  local copies, waits for them, and re-layouts  8.98 us (4%)
  other arithmetic  5.92 us (3%)
    pallas_call x1, Pallas kernels, through_experts(): pl.pallas_call(experts_kernel, out_shape=jax.ShapeDtypeStruct((slots, col...  93.2 us
    all_gather x1, waiting for transfers between devices, per_device(): weight = lax.all_gather(out_weight, 'sp', axis=1, tiled=True)  34.8 us
    pallas_call x1, Pallas kernels, entering_states(): pl.pallas_call(chain_kernel, out_shape=jax.ShapeDtypeStruct(update.shape,...  20.7 us
    pallas_call x1, Pallas kernels, gather_heads(): pl.pallas_call(gather_kernel, out_shape=jax.ShapeDtypeStruct(whole, part....  11.6 us
    unnamed x40, local copies, waits for them, and re-layouts  4.53 us
  transfers between devices with their start and end apart: 1, of which 1 were waited for; matrix products, arithmetic and copies ran while one was open for 9% of the time, Pallas kernels for 16%

commit v1 on v0

--- a/solution.py
+++ b/solution.py
@@ -512,6 +512,18 @@
     return (rot_queries, rot_keys, value_heads)
 
 
+def spread_weight(block):
+    count, me = lax.axis_size("sp"), lax.axis_index("sp")
+    chips = count // 2
+    mine = [(me, block)]
+    for k in range(1, chips):
+        pairs = [(s, (s + 2 * k) % count) for s in range(count)]
+        mine.append(((me - 2 * k) % count, lax.ppermute(block, "sp", pairs)))
+    swap = [(s, s ^ 1) for s in range(count)]
+    other = [(source ^ 1, lax.ppermute(got, "sp", swap)) for source, got in mine]
+    return mine + other
+
+
 def per_device(
     residual,
     query_small,
@@ -532,6 +544,7 @@
 ):
     row_count = residual.shape[0]
     head_count = log_decay.shape[2]
+    weight_blocks = spread_weight(out_weight)
     positions = (lax.axis_index("sp") * row_count + jnp.arange(row_count, dtype=jnp.int32)).astype(
         jnp.float32
     )
@@ -555,11 +568,14 @@
     output_a = final_result(query_a, decay_sum_a, within_a, state_a, gates[:, 0], head_gain[0])
     output_b = final_result(query_b, decay_sum_b, within_b, state_b, gates[:, 1], head_gain[1])
     gathered = gather_heads(jnp.stack([output_a, output_b], axis=0), n_tp)
-    weight = lax.all_gather(out_weight, "sp", axis=1, tiled=True)
-    mixed = (
-        jnp.dot(gathered[0], weight[0], preferred_element_type=jnp.float32)
-        + jnp.dot(gathered[1], weight[1], preferred_element_type=jnp.float32)
-    ).astype(jnp.bfloat16)
+    held = out_weight.shape[1]
+    me = lax.axis_index("sp")
+    total = jnp.zeros((row_count, out_weight.shape[2]), jnp.float32)
+    for source, block in weight_blocks:
+        for g in range(2):
+            part = lax.dynamic_slice_in_dim(gathered[g], source * held, held, axis=1)
+            total = total + jnp.dot(part, block[g], preferred_element_type=jnp.float32)
+    mixed = total.astype(jnp.bfloat16)
     stream = residual.astype(jnp.float32) + mixed.astype(jnp.float32)
     experts = lax.axis_size("sp")
     capacity = 4 * row_count // experts

time: 202 us -> 237 us (1.17)
  Pallas kernels: 125 us -> 196 us
  waiting for transfers between devices: 35.5 us -> 0.02 us
  between operations: 14 us -> 0.8 us
  starting transfers between devices: 0.01 us -> 6.75 us
  matrix products: 11.1 us -> 16.8 us
    pallas_call x1, Pallas kernels: 20.7 us -> 60.4 us  [entering_states(): pl.pallas_call(chain_kernel, out_shape=jax.ShapeDtypeStruct(update.shape,...]
    all_gather x1 -> x0, waiting for transfers between devices: 34.8 us -> none  [per_device(): weight = lax.all_gather(out_weight, 'sp', axis=1, tiled=True)]
    pallas_call x1, Pallas kernels: 93.2 us -> 124 us  [through_experts(): pl.pallas_call(experts_kernel, out_shape=jax.ShapeDtypeStruct((slots, col...]
    ppermute x0 -> x7, starting transfers between devices: none -> 6.75 us  [the longest x3 4.59 us: spread_weight(): mine.append(((me - 2 * k) % count, lax.ppermute(block, 'sp', pairs)))]
    dot_general x2 -> x16, matrix products: 6.01 us -> 12.4 us  [per_device(): total = total + jnp.dot(part, block[g], preferred_element_type=jnp.float32)]
  transfers between devices with their start and end apart: 1 -> 7, of which waited for: 1 -> 0; matrix products, arithmetic and copies ran while one was open for 9% -> 13% of each run, Pallas kernels for 16% -> 31%
where the time goes in v1:
time: 237 us; the launch traced here: 235 us
  Pallas kernels  196 us (83%)
  matrix products  16.8 us (7%)
  local copies, waits for them, and re-layouts  10.3 us (4%)
  starting transfers between devices  6.75 us (3%)
  other arithmetic  4.58 us (2%)
    pallas_call x1, Pallas kernels, through_experts(): pl.pallas_call(experts_kernel, out_shape=jax.ShapeDtypeStruct((slots, col...  124 us
    pallas_call x1, Pallas kernels, entering_states(): pl.pallas_call(chain_kernel, out_shape=jax.ShapeDtypeStruct(update.shape,...  60.4 us
    dot_general x16, matrix products, per_device(): total = total + jnp.dot(part, block[g], preferred_element_type=jnp.float32)  12.4 us
    pallas_call x1, Pallas kernels, gather_heads(): pl.pallas_call(gather_kernel, out_shape=jax.ShapeDtypeStruct(whole, part....  11.5 us
  transfers between devices with their start and end apart: 7, of which 0 were waited for; matrix products, arithmetic and copies ran while one was open for 13% of the time, Pallas kernels for 31%

profile of v1, /device:TPU:1, one launch (start us, length us, event | category | flops | bytes accessed | tf_op | source)
XLA Modules:
  0.0 235.3 jit_solution(2572961812704728238)
XLA Ops:
  0.0 4.1 %collective-permute-start.2 = (bf16[2,256,1024]{2,1,0:T(8,128)(2,1)}, bf16[2,256,1024]{2,1,0:T(8,128)(2,1)}, u32[]{:S(2)}, u32[]{:S(2)}) collective-permute-start(bf16[2,256,1024]{2,1,0:T(8,128)(2,1)} %param.25), channel_id=1, source_target_pairs={{0,24},{4,28},{8,0},{12,4},{16,8},{20,12},{24,16},{28,20},{1,25},{... | collective-permute-start | bytes 3145736 | tf_op jit(solution)/shard_map/ppermute | solution.py:521
  4.1 0.5 collective-permute-start
  4.6 1.5 collective-permute-start.3
  6.1 0.7 slice_bitcast_fusion.33
  7.5 0.8 copy.156
  8.6 1.1 copy.131
  10.0 1.1 copy.145
  11.6 0.4 fusion.135
  15.0 0.4 fusion.42
  15.4 0.9 pad_maximum_fusion.update_ref
  16.4 0.7 broadcast_in_dim.39.fall_ref
  17.1 60.4 %shard_map.154 = bf16[12,128,128]{2,1,0:T(8,128)(2,1)} custom-call(f32[12,128,128]{2,1,0:T(8,128)} %pad_maximum_fusion.update_ref, f32[12,1,128]{2,1,0:T(1,128)} %broadcast_in_dim.39.fall_ref), custom_call_target="tpu_custom_call" | custom-call | tf_op jit(solution)/shard_map/pallas_call | solution.py:89
  77.6 0.4 convolution_bitcast_fusion.3
  78.0 1.2 multiply_reduce_fusion.1
  79.2 0.4 fusion.134
  80.2 0.4 convolution_bitcast_fusion.2
  81.3 0.7 pad_maximum_fusion.2.part_ref
  82.1 11.5 %shard_map.155 = bf16[2,128,2048]{2,1,0:T(8,128)(2,1)} custom-call(bf16[2,128,512]{2,1,0:T(8,128)(2,1)} %pad_maximum_fusion.2.part_ref), custom_call_target="tpu_custom_call" | custom-call | tf_op jit(solution)/shard_map/pallas_call | solution.py:130
  93.6 1.3 fusion.133
  94.9 0.6 reduce-window.6
  97.2 0.5 collective-permute-start.4
  97.8 1.3 fusion.31
  99.1 1.3 fusion.32
  100.3 1.3 fusion.33
  101.6 1.3 fusion.34
  102.9 1.3 fusion.29
  104.2 1.3 fusion.30
  105.5 1.3 fusion.35
  106.8 1.5 fusion.11
  109.5 0.3 fusion.16.stream_ref
  109.9 124.0 %shard_map.156 = bf16[512,1024]{1,0:T(8,128)(2,1)S(1)} custom-call(f32[128,1024]{1,0:T(8,128)S(1)} %fusion.16.stream_ref, f32[1,1024]{1,0:T(1,128)S(1)} %bitcast.174, bf16[512,128]{1,0:T(8,128)(2,1)S(1)} %convert_bitcast_fusion.select_ref, bf16[1,4096,512]{2,1,0:T(8,128)(2,1)} %gate_hbm.1, bf16[1,4096,512]{2,1,0:T(8,128)(2,1)} %up_hbm.1, ...), custom_call_target="tpu_custom_call" | custom-call | tf_op jit(solution)/shard_map/pallas_call | solution.py:407
  234.3 1.0 fusion.17
  (111 shorter events, 9.0 us)
Async XLA Ops:
  0.0 11.6 %copy-start.2 = (bf16[128,2,512]{2,1,0:T(2,128)(2,1)S(1)}, bf16[128,2,512]{2,1,0:T(2,128)(2,1)}, u32[]{:S(2)}) copy-start(bf16[128,2,512]{2,1,0:T(2,128)(2,1)} %param.21) | copy-start | bytes 786436
  0.0 12.8 %copy-start.5 = (bf16[128,512]{1,0:T(8,128)(2,1)S(1)}, bf16[128,512]{1,0:T(8,128)(2,1)}, u32[]{:S(2)}) copy-start(bf16[128,512]{1,0:T(8,128)(2,1)} %param.17) | copy-start | bytes 393220
  0.0 97.7 %collective-permute-start.2 = (bf16[2,256,1024]{2,1,0:T(8,128)(2,1)}, bf16[2,256,1024]{2,1,0:T(8,128)(2,1)}, u32[]{:S(2)}, u32[]{:S(2)}) collective-permute-start(bf16[2,256,1024]{2,1,0:T(8,128)(2,1)} %param.25), channel_id=1, source_target_pairs={{0,24},{4,28},{8,0},{12,4},{16,8},{20,12},{24,16},{28,20},{1,25},{... | collective-permute-start | bytes 3145736 | tf_op jit(solution)/shard_map/ppermute | solution.py:521
  4.1 93.0 %collective-permute-start.1 = (bf16[2,256,1024]{2,1,0:T(8,128)(2,1)}, bf16[2,256,1024]{2,1,0:T(8,128)(2,1)}, u32[]{:S(2)}, u32[]{:S(2)}) collective-permute-start(bf16[2,256,1024]{2,1,0:T(8,128)(2,1)} %param.25), channel_id=1, source_target_pairs={{0,16},{4,20},{8,24},{12,28},{16,0},{20,4},{24,8},{28,12},{1,17},{... | collective-permute-start | bytes 3145736 | tf_op jit(solution)/shard_map/ppermute | solution.py:521
  4.1 93.0 %collective-permute-start = (bf16[2,256,1024]{2,1,0:T(8,128)(2,1)}, bf16[2,256,1024]{2,1,0:T(8,128)(2,1)}, u32[]{:S(2)}, u32[]{:S(2)}) collective-permute-start(bf16[2,256,1024]{2,1,0:T(8,128)(2,1)} %param.25), channel_id=1, source_target_pairs={{0,8},{4,12},{8,16},{12,20},{16,24},{20,28},{24,0},{28,4},{1,9},{5... | collective-permute-start | bytes 3145736 | tf_op jit(solution)/shard_map/ppermute | solution.py:521
  4.6 98.3 %collective-permute-start.3 = (bf16[2,256,1024]{2,1,0:T(8,128)(2,1)}, bf16[2,256,1024]{2,1,0:T(8,128)(2,1)}, u32[]{:S(2)}, u32[]{:S(2)}) collective-permute-start(bf16[2,256,1024]{2,1,0:T(8,128)(2,1)} %param.25), channel_id=1, source_target_pairs={{0,4},{4,0},{8,12},{12,8},{16,20},{20,16},{24,28},{28,24},{1,5},{5... | collective-permute-start | bytes 3145736 | tf_op jit(solution)/shard_map/ppermute | solution.py:523
  9.7 3.5 %copy-start.6 = (bf16[128,512]{1,0:T(8,128)(2,1)S(1)}, bf16[128,512]{1,0:T(8,128)(2,1)}, u32[]{:S(2)}) copy-start(bf16[128,512]{1,0:T(8,128)(2,1)} %param.18) | copy-start | bytes 393220
  14.9 64.3 %copy-start.3 = (bf16[128,2,512]{2,1,0:T(2,128)(2,1)S(1)}, bf16[128,2,512]{2,1,0:T(2,128)(2,1)}, u32[]{:S(2)}) copy-start(bf16[128,2,512]{2,1,0:T(2,128)(2,1)} %param.22) | copy-start | bytes 786436
  15.4 64.4 %copy-start.8 = (f32[2,512]{1,0:T(2,128)S(1)}, f32[2,512]{1,0:T(2,128)}, u32[]{:S(2)}) copy-start(f32[2,512]{1,0:T(2,128)} %param.24) | copy-start | bytes 12292
  77.6 3.1 %slice-start = ((bf16[12,128,128]{2,1,0:T(8,128)(2,1)}), bf16[8,128,128]{2,1,0:T(8,128)(2,1)S(1)}, s32[]{:S(2)}) async-start(bf16[12,128,128]{2,1,0:T(8,128)(2,1)} %shard_map.154), calls=%async_computation | async-start | bytes 524288 | tf_op jit(solution)/shard_map/slice | solution.py:567
  80.1 15.9 %copy-start.7 = (s32[128,2]{0,1:T(2,128)S(1)}, s32[128,2]{0,1:T(2,128)}, u32[]{:S(2)}) copy-start(s32[128,2]{0,1:T(2,128)} %param.27) | copy-start | bytes 3076
  80.6 15.9 %copy-start.1 = (bf16[2,256,1024]{2,1,0:T(8,128)(2,1)S(1)}, bf16[2,256,1024]{2,1,0:T(8,128)(2,1)}, u32[]{:S(2)}) copy-start(bf16[2,256,1024]{2,1,0:T(8,128)(2,1)} %param.25) | copy-start | bytes 3145732
  81.2 15.8 %copy-start.9 = (f32[128,2]{0,1:T(2,128)S(1)}, f32[128,2]{0,1:T(2,128)}, u32[]{:S(2)}) copy-start(f32[128,2]{0,1:T(2,128)} %param.28) | copy-start | bytes 3076
  97.1 11.2 %collective-permute-start.5 = (bf16[2,256,1024]{2,1,0:T(8,128)(2,1)}, bf16[2,256,1024]{2,1,0:T(8,128)(2,1)S(1)}, u32[]{:S(2)}, u32[]{:S(2)}) collective-permute-start(bf16[2,256,1024]{2,1,0:T(8,128)(2,1)} %collective-permute-done.1), channel_id=1, source_target_pairs={{0,4},{4,0},{8,12},{12,8},{16,20},{20,16},{24,28},{28,24},{1,5},{5... | collective-permute-start | bytes 3145736 | tf_op jit(solution)/shard_map/ppermute | solution.py:523
  97.2 12.1 %collective-permute-start.4 = (bf16[2,256,1024]{2,1,0:T(8,128)(2,1)}, bf16[2,256,1024]{2,1,0:T(8,128)(2,1)S(1)}, u32[]{:S(2)}, u32[]{:S(2)}) collective-permute-start(bf16[2,256,1024]{2,1,0:T(8,128)(2,1)} %collective-permute-done), channel_id=1, source_target_pairs={{0,4},{4,0},{8,12},{12,8},{16,20},{20,16},{24,28},{28,24},{1,5},{5... | collective-permute-start | bytes 3145736 | tf_op jit(solution)/shard_map/ppermute | solution.py:523
  97.7 11.1 %collective-permute-start.6 = (bf16[2,256,1024]{2,1,0:T(8,128)(2,1)}, bf16[2,256,1024]{2,1,0:T(8,128)(2,1)S(1)}, u32[]{:S(2)}, u32[]{:S(2)}) collective-permute-start(bf16[2,256,1024]{2,1,0:T(8,128)(2,1)} %collective-permute-done.2), channel_id=1, source_target_pairs={{0,4},{4,0},{8,12},{12,8},{16,20},{20,16},{24,28},{28,24},{1,5},{5... | collective-permute-start | bytes 3145736 | tf_op jit(solution)/shard_map/ppermute | solution.py:523
  106.8 2.7 %copy-start.4 = (bf16[128,1024]{1,0:T(8,128)(2,1)S(1)}, bf16[128,1024]{1,0:T(8,128)(2,1)}, u32[]{:S(2)}) copy-start(bf16[128,1024]{1,0:T(8,128)(2,1)} %param.16) | copy-start | bytes 786436
  108.8 1.1 copy-start

commit v2 on v0

v2 whole, which is shorter than its diff:
```python
import jax
import jax.numpy as jnp
from jax import lax
from jax.experimental import pallas as pl
from jax.experimental.pallas import tpu as pltpu
from jax.sharding import PartitionSpec as P

MESH = pl.DeviceIdType.MESH


EPS = 1e-06
THETA = 10000.0


def greet(axes):
    barrier = pltpu.get_barrier_semaphore()
    total = 0
    for axis in axes:
        count, me = lax.axis_size(axis), lax.axis_index(axis)

        def signal(k, _, axis=axis, count=count, me=me):
            pl.semaphore_signal(
                barrier, inc=1, device_id={axis: (me + k) % count}, device_id_type=MESH
            )
            return 0

        lax.fori_loop(1, count, signal, 0)
        total += count - 1
    pl.semaphore_wait(barrier, total)


def remote(source, target, send_sem, recv_sem, axis, index):
    return pltpu.make_async_remote_copy(
        src_ref=source,
        dst_ref=target,
        send_sem=send_sem,
        recv_sem=recv_sem,
        device_id={axis: index},
        device_id_type=MESH,
    )


GROUPS = 4


def grid_of(count):
    across = max(k for k in range(1, count + 1) if count % k == 0 and k * k <= count)
    return across, count // across


def group_order():
    middle = (GROUPS - 1) / 2
    return sorted(range(GROUPS), key=lambda g: (abs(g - middle), g))


def turned(block, cosine, sine):
    half = block.shape[1] // 2
    if half % 128:
        swapped = pltpu.roll(block, half, axis=1)
    else:
        swapped = jnp.concatenate([block[:, half:], block[:, :half]], axis=1)
    return block * cosine + swapped * sine


def layer_kernel(
    residual_ref,
    query_a_ref,
    key_a_ref,
    query_b_ref,
    key_b_ref,
    values_ref,
    gates_ref,
    cos_a_ref,
    sin_a_ref,
    cos_b_ref,
    sin_b_ref,
    cumul_ref,
    cumul_rows_ref,
    head_gain_ref,
    gain_ref,
    target_ref,
    weight_hbm,
    gate_hbm,
    up_hbm,
    down_hbm,
    out_ref,
    stream_ref,
    rot_queries_a,
    rot_queries_b,
    within,
    update,
    fall,
    held,
    departing,
    heads,
    w_out,
    mix,
    w_gate,
    w_up,
    w_down,
    squares,
    outgoing,
    arrived,
    hidden,
    result,
    returned,
    acc_a,
    acc_b,
    acc_c,
    load_sem,
    chain_send,
    chain_recv,
    heads_send,
    heads_recv,
    w_line_send,
    w_pair_send,
    w_recv,
    sq_send,
    sq_recv,
    disp_send,
    disp_recv,
    fwd_send,
    fwd_recv,
    fwd_relay_send,
    fwd_relay_recv,
    hid_send,
    hid_recv,
    hid_relay_send,
    hid_relay_recv,
    ret_send,
    ret_recv,
):
    n_sp, n_tp = lax.axis_size("sp"), lax.axis_size("tp")
    s, t = lax.axis_index("sp"), lax.axis_index("tp")
    bf16, f32 = jnp.bfloat16, jnp.float32
    per_group = n_sp // GROUPS
    order = group_order()
    across, down = grid_of(n_tp)
    x, y = t % across, t // across
    cap = outgoing.shape[0] // n_sp
    cols = stream_ref.shape[1]
    units = w_gate.shape[1]
    count = stream_ref.shape[0]
    chips = n_sp // 2
    z, core = s // 2, s % 2
    loads = [
        pltpu.make_async_copy(source.at[0], target, load_sem.at[i])
        for i, (source, target) in enumerate(
            ((gate_hbm, w_gate), (up_hbm, w_up), (down_hbm, w_down))
        )
    ]
    own_load = pltpu.make_async_copy(weight_hbm, w_out.at[s], load_sem.at[3])
    own_load.start()
    for load in loads:
        load.start()
    greet(("sp", "tp"))

    partner = s + 1 - 2 * core
    ahead = s + 2 - 4 * core
    has_ahead = jnp.where(core == 0, z < chips - 1, z > 0)

    def along_line(b):
        return remote(w_out.at[b], w_out.at[b], w_line_send.at[b], w_recv.at[b], "sp", ahead)

    def to_partner(b):
        return remote(w_out.at[b], w_out.at[b], w_pair_send.at[b], w_recv.at[b], "sp", partner)

    def pass_on(b):
        @pl.when(has_ahead)
        def _():
            along_line(b).start()

    own_load.wait()
    to_partner(s).start()
    pass_on(s)

    def chip_behind(j):
        return z + (2 * core - 1) * j

    def serve(j, i):
        chip = chip_behind(j)

        @pl.when((chip >= 0) & (chip < chips))
        def _():
            b = chip * 2 + i
            along_line(b).wait_recv()
            to_partner(b).start()
            pass_on(b)

    head_count = cumul_ref.shape[1] // 2
    groups = (
        (query_a_ref, key_a_ref, cos_a_ref, sin_a_ref, rot_queries_a),
        (query_b_ref, key_b_ref, cos_b_ref, sin_b_ref, rot_queries_b),
    )
    size_a = query_a_ref.shape[1] // head_count
    dv = values_ref.shape[2] // head_count
    rows_i = lax.broadcasted_iota(jnp.int32, (count, count), 0)
    rows_j = lax.broadcasted_iota(jnp.int32, (count, count), 1)
    causal = rows_i >= rows_j

    def hop(c):
        return remote(
            departing.at[c], held.at[c], chain_send.at[c], chain_recv.at[c], "sp", (s + 1) % n_sp
        )

    pieces_of = []
    total_pieces = 0
    for g, (query_ref, key_ref, cos_ref, sin_ref, rot_ref) in enumerate(groups):
        size = query_ref.shape[1] // head_count
        for h in range(head_count):
            i = g * head_count + h
            lanes = slice(h * size, (h + 1) * size)
            cosine, sine = cos_ref[...], sin_ref[...]
            rot_q = turned(query_ref[:, lanes].astype(f32), cosine, sine).astype(bf16)
            rot_k = (turned(key_ref[:, lanes].astype(f32), cosine, sine) * size ** (-0.5)).astype(
                bf16
            )
            rot_ref[:, lanes] = rot_q
            column, row = cumul_ref[:, i : i + 1], cumul_rows_ref[i : i + 1, :]
            scores = lax.dot_general(
                rot_q, rot_k, (((1,), (1,)), ((), ())), preferred_element_type=f32
            )
            spread = column - row
            weight = jnp.where(causal, jnp.exp(jnp.where(causal, spread, 0.0)), 0.0)
            value = values_ref[g, :, h * dv : (h + 1) * dv]
            within[i] = jnp.dot(
                (scores * weight).astype(bf16), value, preferred_element_type=f32
            )
            last = cumul_ref[count - 1 : count, i : i + 1]
            carried = (rot_k.astype(f32) * jnp.exp(last - column)).astype(bf16)
            grown = lax.dot_general(
                carried, value, (((0,), (0,)), ((), ())), preferred_element_type=f32
            )
            mine = []
            for c in range(size // size_a):
                update[total_pieces] = grown[c * size_a : (c + 1) * size_a]
                fall[total_pieces] = jnp.broadcast_to(jnp.exp(last), (1, dv))
                mine.append(total_pieces)
                total_pieces += 1
            pieces_of.append(mine)

    to_line = partner
    to_partner(partner).wait_recv()
    pass_on(to_line)

    def step(c, _):
        @pl.when(s == 0)
        def _():
            held[c] = jnp.zeros(held.shape[1:], held.dtype)

        @pl.when(s > 0)
        def _():
            hop(c).wait_recv()

        @pl.when(s < n_sp - 1)
        def _():
            departing[c] = (fall[c] * held[c].astype(f32) + update[c]).astype(bf16)
            hop(c).start()

        return 0

    lax.fori_loop(0, total_pieces, step, 0)

    serve(1, 0)

    def heads_copy(g, k, source):
        block = heads.at[source, g]
        return remote(
            block, block, heads_send.at[g, k], heads_recv.at[g, source], "tp", (t + k) % n_tp
        )

    for g, (query_ref, _, _, _, rot_ref) in enumerate(groups):
        size = query_ref.shape[1] // head_count
        for h in range(head_count):
            i = g * head_count + h
            retained = within[i]
            cross = jnp.zeros((count, dv), f32)
            for c, piece in enumerate(pieces_of[i]):
                lanes = slice(h * size + c * size_a, h * size + (c + 1) * size_a)
                cross = cross + jnp.dot(rot_ref[:, lanes], held[piece], preferred_element_type=f32)
            retained = retained + cross * jnp.exp(cumul_ref[:, i : i + 1])
            scaled = retained * lax.rsqrt(
                jnp.mean(retained * retained, axis=1, keepdims=True) + EPS
            )
            lanes = slice(h * dv, (h + 1) * dv)
            gated = jax.nn.silu(gates_ref[g, :, lanes].astype(f32))
            heads[t, g, :, lanes] = (scaled * head_gain_ref[g : g + 1, lanes] * gated).astype(bf16)

        def heads_start(k, _, g=g):
            heads_copy(g, k, t).start()
            return 0

        lax.fori_loop(1, n_tp, heads_start, 0)

    serve(1, 1)
    for g in range(2):

        def heads_wait(k, _, g=g):
            heads_copy(g, k, (t + k) % n_tp).wait_recv()
            return 0

        lax.fori_loop(1, n_tp, heads_wait, 0)

    held_rows = w_out.shape[2]
    ratio = n_sp // n_tp

    def project_lanes(b, lanes):
        part = jnp.dot(heads[b // ratio, 0, :, lanes], w_out[b, 0], preferred_element_type=f32)
        part += jnp.dot(heads[b // ratio, 1, :, lanes], w_out[b, 1], preferred_element_type=f32)
        mix[...] += part

    def project(b):
        if held_rows % 128 == 0:
            project_lanes(
                b, pl.ds(pl.multiple_of((b % ratio) * held_rows, held_rows), held_rows)
            )
            return
        for r in range(ratio):

            @pl.when(b % ratio == r)
            def _(r=r):
                project_lanes(b, slice(r * held_rows, (r + 1) * held_rows))

    mix[...] = jnp.zeros_like(mix)
    for i in range(2):
        project(z * 2 + i)

    def project_chips(j, served):
        for i in range(2):
            if not served:
                serve(j, i)
        chip = chip_behind(j)

        @pl.when((chip >= 0) & (chip < chips))
        def _():
            for i in range(2):
                project(chip * 2 + i)

        other = z - (2 * core - 1) * j

        @pl.when((other >= 0) & (other < chips))
        def _():
            for i in range(2):
                to_partner(other * 2 + i).wait_recv()
                project(other * 2 + i)

    def project_far(j, _):
        project_chips(j, False)
        return 0

    def rows_of(p):
        return pl.ds(pl.multiple_of(p * cap, cap), cap)

    def group_rows(g, part=None):
        size = per_group * cap
        start = order[g] * size
        if part is None:
            return pl.ds(start, size)
        return pl.ds(start + part * (size // 2), size // 2)

    def square_copy(k, source):
        block, other = squares.at[source], (t + k) % n_tp
        return remote(block, block, sq_send.at[k], sq_recv.at[source], "tp", other)

    def dispatch(p, q):
        return remote(
            outgoing.at[rows_of(p)],
            arrived.at[t, rows_of(q)],
            disp_send.at[p],
            disp_recv.at[q],
            "sp",
            p,
        )

    def members(g, action):
        def body(j, _):
            action(order[g] * per_group + j)
            return 0

        lax.fori_loop(0, per_group, body, 0)

    def others(g, action):
        def guarded(p):
            @pl.when(p != s)
            def _():
                action(p)

        members(g, guarded)

    def finish_rows():
        stream = residual_ref[...].astype(f32) + mix[...].astype(bf16).astype(f32)
        stream_ref[...] = stream
        own = jnp.sum(stream * stream, axis=1, keepdims=True)
        squares[t] = jnp.broadcast_to(own, (count, count)).T[0:8, :]

        def square_start(k, _):
            square_copy(k, t).start()
            return 0

        def square_wait(k, _):
            square_copy(k, (t + k) % n_tp).wait()
            return 0

        lax.fori_loop(1, n_tp, square_start, 0)
        lax.fori_loop(1, n_tp, square_wait, 0)
        total = squares[0]
        for p in range(1, n_tp):
            total = total + squares[p]
        scale = lax.rsqrt(total[0:1, :] / (cols * n_tp) + EPS)
        scale = jnp.broadcast_to(scale, (count, count)).T[:, 0:1]
        normed = (stream_ref[...] * scale * gain_ref[...]).astype(bf16)
        slots = lax.broadcasted_iota(jnp.int32, (outgoing.shape[0], count), 0)
        select = (slots == target_ref[0:1, :]) | (slots == target_ref[1:2, :])
        select = jnp.where(select, 1.0, 0.0).astype(bf16)
        outgoing[...] = jnp.dot(select, normed, preferred_element_type=f32).astype(bf16)
        for g in range(GROUPS):
            others(g, lambda p: dispatch(p, s).start())
        arrived[t, rows_of(s)] = outgoing[rows_of(s)]

    lines = (
        [y * across + (x + k) % across for k in range(1, across)],
        [((y + k) % down) * across + x for k in range(1, down)],
    )
    direct = lines[0] + lines[1]

    def straight(buffer, sems, g, i, source, rows):
        block = buffer.at[source, rows]
        return remote(block, block, sems[0].at[g, i], sems[1].at[g, source], "tp", direct[i])

    def relayed(buffer, sems, g, part, i, source, target):
        block = buffer.at[source, group_rows(g, part)]
        return remote(
            block, block, sems[2].at[g, part, i], sems[3].at[g, source, part], "tp", target
        )

    def relay(buffer, sems, g):
        for part in range(2):
            for k, source in enumerate(lines[part]):
                i = k if part == 0 else len(lines[0]) + k
                straight(buffer, sems, g, i, source, group_rows(g)).wait_recv()
                for j, target in enumerate(lines[1 - part]):
                    relayed(
                        buffer, sems, g, part, k * len(lines[1 - part]) + j, source, target
                    ).start()

    def place_of(k):
        return ((y + k // across) % down) * across + (x + k % across) % across

    def wait_relayed(buffer, sems, g, k):
        @pl.when((k // across) * (k % across) > 0)
        def _():
            source = place_of(k)
            for part in range(2):
                relayed(buffer, sems, g, part, 0, source, source).wait_recv()

    def finish_sends(buffer, sems, g):
        for i in range(len(direct)):
            straight(buffer, sems, g, i, t, group_rows(g)).wait_send()
        for part in range(2):
            for i in range(len(lines[0]) * len(lines[1])):
                relayed(buffer, sems, g, part, i, t, direct[0]).wait_send()

    arrived_sems = (fwd_send, fwd_recv, fwd_relay_send, fwd_relay_recv)
    hidden_sems = (hid_send, hid_recv, hid_relay_send, hid_relay_recv)

    def forward(g):
        def block(p):
            @pl.when(p != s)
            def _():
                dispatch(p, p).wait_recv()

            for i in range(len(direct)):
                straight(arrived, arrived_sems, g, i, t, rows_of(p)).start()

        members(g, block)

    def through_units(g):
        acc_a[...] = jnp.zeros_like(acc_a)
        acc_b[...] = jnp.zeros_like(acc_b)

        def body(k, _):
            wait_relayed(arrived, arrived_sems, g, k)
            p = place_of(k)
            part = pl.ds(pl.multiple_of(p * cols, cols), cols)
            rows = arrived[p, group_rows(g)]
            acc_a[...] += jnp.dot(rows, w_gate[part, :], preferred_element_type=f32)
            acc_b[...] += jnp.dot(rows, w_up[part, :], preferred_element_type=f32)
            return 0

        lax.fori_loop(0, n_tp, body, 0)
        hidden[t, group_rows(g)] = (jax.nn.silu(acc_a[...]) * acc_b[...]).astype(bf16)
        for i in range(len(direct)):
            straight(hidden, hidden_sems, g, i, t, group_rows(g)).start()

    def give_back(p, q):
        return remote(
            result.at[rows_of(p)], returned.at[rows_of(q)], ret_send.at[p], ret_recv.at[q], "sp", p
        )

    def through_down(g):
        acc_c[...] = jnp.zeros_like(acc_c)

        def body(k, _):
            wait_relayed(hidden, hidden_sems, g, k)
            p = place_of(k)
            part = pl.ds(pl.multiple_of(p * units, units), units)
            acc_c[...] += jnp.dot(
                hidden[p, group_rows(g)], w_down[part, :], preferred_element_type=f32
            )
            return 0

        lax.fori_loop(0, n_tp, body, 0)
        result[group_rows(g)] = acc_c[...].astype(bf16)
        others(g, lambda p: give_back(p, s).start())

    relay_rows = lambda g: relay(arrived, arrived_sems, g)
    relay_hidden = lambda g: relay(hidden, hidden_sems, g)

    inner_lo, inner_hi = chips // 4, chips - chips // 4
    inner = (z >= inner_lo) & (z < inner_hi)
    if chips > 1:
        project_chips(1, True)
    lax.fori_loop(2, inner_hi, project_far, 0)

    @pl.when(inner)
    def _():
        finish_rows()

    half = GROUPS // 2
    for g in range(half):
        forward(g)
    for g in range(half):
        relay_rows(g)
    for load in loads:
        load.wait()
    for g in range(half):
        through_units(g)

    lax.fori_loop(inner_hi, chips, project_far, 0)

    @pl.when(jnp.logical_not(inner))
    def _():
        finish_rows()

    for g in range(half):
        relay_hidden(g)
    for g in range(half):
        through_down(g)
    for g in range(half, GROUPS):
        forward(g)
    for g in range(half, GROUPS):
        relay_rows(g)
    for g in range(half, GROUPS):
        through_units(g)
    for g in range(half, GROUPS):
        relay_hidden(g)
    for g in range(half, GROUPS):
        through_down(g)

    returned[rows_of(s)] = result[rows_of(s)]
    for g in range(GROUPS):
        others(g, lambda p: give_back(p, p).wait_recv())
    out_ref[...] = returned[...]

    @pl.when(s < n_sp - 1)
    def _():
        def gone(c, _):
            hop(c).wait_send()
            return 0

        lax.fori_loop(0, total_pieces, gone, 0)

    for g in range(2):

        def heads_gone(k, _, g=g):
            heads_copy(g, k, t).wait_send()
            return 0

        lax.fori_loop(1, n_tp, heads_gone, 0)

    def passed(j, _):
        chip = chip_behind(j)

        @pl.when((chip >= 0) & (chip < chips))
        def _():
            for i in range(2):
                b = chip * 2 + i

                @pl.when(has_ahead)
                def _():
                    along_line(b).wait_send()

                @pl.when((b == s) | (j > 0))
                def _():
                    to_partner(b).wait_send()

        return 0

    lax.fori_loop(0, chips, passed, 0)
    for g in range(GROUPS):
        others(g, lambda p: dispatch(p, s).wait_send())
        others(g, lambda p: give_back(p, s).wait_send())
        finish_sends(arrived, arrived_sems, g)
        finish_sends(hidden, hidden_sems, g)


def tables(positions, size):
    half = size // 2
    inverse = jnp.power(THETA, -jnp.arange(half, dtype=jnp.float32) * 2.0 / size)
    inverse = jnp.concatenate([inverse, inverse])
    sign = jnp.where(jnp.arange(size) < half, -1.0, 1.0)
    angles = positions[:, None] * inverse[None, :]
    return jnp.cos(angles), jnp.sin(angles) * sign[None, :]


def per_device(
    residual,
    query_small,
    key_narrow_group,
    query_large,
    key_large,
    values,
    gates,
    log_decay,
    head_gain,
    out_weight,
    norm_gain,
    routes,
    route_weight,
    expert_gate,
    expert_up,
    expert_down,
):
    n_sp, n_tp = lax.axis_size("sp"), lax.axis_size("tp")
    row_count, cols = residual.shape
    head_count = log_decay.shape[2]
    bf16, f32 = jnp.bfloat16, jnp.float32
    positions = (lax.axis_index("sp") * row_count + jnp.arange(row_count, dtype=jnp.int32)).astype(
        f32
    )
    size_a, size_b = query_small.shape[1] // head_count, query_large.shape[1] // head_count
    cos_a, sin_a = tables(positions, size_a)
    cos_b, sin_b = tables(positions, size_b)
    cumul = jnp.cumsum(log_decay.reshape(row_count, 2 * head_count), axis=0)

    experts = n_sp
    capacity = 4 * row_count // experts
    slots = experts * capacity
    numbers = jnp.arange(experts, dtype=jnp.int32)
    named = [(routes[:, c][:, None] == numbers[None, :]) for c in range(2)]
    counted = (named[0].astype(bf16) + named[1].astype(bf16))
    earlier = jnp.arange(row_count)[:, None] > jnp.arange(row_count)[None, :]
    before = jnp.dot(earlier.astype(bf16), counted, preferred_element_type=f32)
    target = [
        routes[:, c] * capacity
        + jnp.sum(jnp.where(named[c], before, 0.0), axis=1).astype(jnp.int32)
        for c in range(2)
    ]

    pieces = head_count * (1 + size_b // size_a)
    value_size = values.shape[2] // head_count
    width, units = expert_gate.shape[1:]
    dma = pltpu.SemaphoreType.DMA
    across, down = grid_of(n_tp)
    straights, relays = across + down - 2, (across - 1) * (down - 1)
    vmem = pl.BlockSpec(memory_space=pltpu.VMEM)
    hbm = pl.BlockSpec(memory_space=pl.ANY)
    returned, stream = pl.pallas_call(
        layer_kernel,
        out_shape=(
            jax.ShapeDtypeStruct((slots, cols), bf16),
            jax.ShapeDtypeStruct((row_count, cols), f32),
        ),
        in_specs=[vmem] * 16 + [hbm] * 4,
        out_specs=(vmem, vmem),
        scratch_shapes=[
            pltpu.VMEM(query_small.shape, bf16),
            pltpu.VMEM(query_large.shape, bf16),
            pltpu.VMEM((2 * head_count, row_count, value_size), f32),
            pltpu.VMEM((pieces, size_a, value_size), f32),
            pltpu.VMEM((pieces, 1, value_size), f32),
            pltpu.VMEM((pieces, size_a, value_size), bf16),
            pltpu.VMEM((pieces, size_a, value_size), bf16),
            pltpu.VMEM((n_tp, 2, row_count, values.shape[2]), bf16),
            pltpu.VMEM((n_sp,) + out_weight.shape, bf16),
            pltpu.VMEM((row_count, cols), f32),
            pltpu.VMEM((width, units), bf16),
            pltpu.VMEM((width, units), bf16),
            pltpu.VMEM(expert_down.shape[1:], bf16),
            pltpu.VMEM((n_tp, 8, row_count), f32),
            pltpu.VMEM((slots, cols), bf16),
            pltpu.VMEM((n_tp, slots, cols), bf16),
            pltpu.VMEM((n_tp, slots, units), bf16),
            pltpu.VMEM((slots, cols), bf16),
            pltpu.VMEM((slots, cols), bf16),
            pltpu.VMEM((slots // GROUPS, units), f32),
            pltpu.VMEM((slots // GROUPS, units), f32),
            pltpu.VMEM((slots // GROUPS, cols), f32),
            dma((4,)),
            dma((pieces,)),
            dma((pieces,)),
            dma((2, n_tp)),
            dma((2, n_tp)),
            dma((n_sp,)),
            dma((n_sp,)),
            dma((n_sp,)),
            dma((n_tp,)),
            dma((n_tp,)),
            dma((n_sp,)),
            dma((n_sp,)),
            dma((GROUPS, straights)),
            dma((GROUPS, n_tp)),
            dma((GROUPS, 2, relays)),
            dma((GROUPS, n_tp, 2)),
            dma((GROUPS, straights)),
            dma((GROUPS, n_tp)),
            dma((GROUPS, 2, relays)),
            dma((GROUPS, n_tp, 2)),
            dma((n_sp,)),
            dma((n_sp,)),
        ],
        compiler_params=pltpu.CompilerParams(
            collective_id=0, has_side_effects=True, vmem_limit_bytes=58 * 2**20
        ),
    )(
        residual,
        query_small,
        key_narrow_group,
        query_large,
        key_large,
        jnp.swapaxes(values, 0, 1),
        jnp.swapaxes(gates, 0, 1),
        cos_a,
        sin_a,
        cos_b,
        sin_b,
        cumul,
        cumul.T,
        head_gain,
        norm_gain[None, :],
        jnp.stack(target),
        out_weight,
        expert_gate,
        expert_up,
        expert_down,
    )
    ids = jnp.arange(slots, dtype=jnp.int32)[None, :]
    picks = [
        jnp.dot(
            (target[c][:, None] == ids).astype(bf16), returned, preferred_element_type=f32
        )
        for c in range(2)
    ]
    routed = route_weight[:, 0:1] * picks[0] + route_weight[:, 1:2] * picks[1]
    return (stream + routed).astype(bf16)


def solution(mesh):
    placed = (
        P("sp", "tp"),
        P("sp", "tp"),
        P("sp", "tp"),
        P("sp", "tp"),
        P("sp", "tp"),
        P("sp", None, "tp"),
        P("sp", None, "tp"),
        P("sp", None, "tp"),
        P(None, "tp"),
        P(None, "sp", "tp"),
        P("tp"),
        P("sp", None),
        P("sp", None),
        P("sp", None, "tp"),
        P("sp", None, "tp"),
        P("sp", None, "tp"),
    )
    return jax.shard_map(
        per_device, mesh=mesh, in_specs=placed, out_specs=P("sp", "tp"), check_vma=False
    )
```

time: 202 us -> 180 us (0.89)
  Pallas kernels: 125 us -> 168 us
  waiting for transfers between devices: 35.5 us -> 0 us
  between operations: 14 us -> 0.06 us
  matrix products: 11.1 us -> 4.13 us
  local copies, waits for them, and re-layouts: 8.98 us -> 4.09 us
  other arithmetic: 5.92 us -> 3.86 us
    pallas_call x3 -> x1, Pallas kernels: 125 us -> 168 us  [per_device(): pl.pallas_call(layer_kernel, out_shape=(jax.ShapeDtypeStruct((slots, cols...]
    all_gather x1 -> x0, waiting for transfers between devices: 34.8 us -> none  [per_device(): weight = lax.all_gather(out_weight, 'sp', axis=1, tiled=True)]
    dot_general x10 -> x3, matrix products: 11.1 us -> 4.13 us  [the longest x2 3.98 us: per_device(): jnp.dot((target[c][:, None] == ids).astype(bf16), returned, preferred_ele...]
    unnamed x40 -> x6, local copies, waits for them, and re-layouts: 4.53 us -> 0.01 us
    mul x0 -> x2, other arithmetic: none -> 2.22 us  [tables(): return (jnp.cos(angles), jnp.sin(angles) * sign[None, :])]
  transfers between devices with their start and end apart: 1 -> 0, of which waited for: 1 -> 0; matrix products, arithmetic and copies ran while one was open for 9% -> 0% of each run, Pallas kernels for 16% -> 0%
where the time goes in v2:
time: 180 us
  Pallas kernels  168 us (93%)
  matrix products  4.13 us (2%)
  local copies, waits for them, and re-layouts  4.09 us (2%)
  other arithmetic  3.86 us (2%)
    pallas_call x1, Pallas kernels, per_device(): pl.pallas_call(layer_kernel, out_shape=(jax.ShapeDtypeStruct((slots, cols...  168 us
    dot_general x2, matrix products, per_device(): jnp.dot((target[c][:, None] == ids).astype(bf16), returned, preferred_ele...  3.98 us

profile of v2, /device:TPU:1, one launch (start us, length us, event | category | flops | bytes accessed | tf_op | source)
XLA Modules:
  0.0 180.2 jit_solution(5972302425259796842)
XLA Ops:
  0.0 0.8 slice_bitcast_fusion.3
  0.8 0.1 select_reduce_fusion.1
  0.9 0.8 bitcast_add_fusion.3
  1.7 0.6 pad_add_fusion.target_ref
  2.3 1.3 fusion.3
  3.5 0.1 compare_select_fusion.1
  3.6 1.0 fusion.6
  4.6 1.9 %copy_bitcast_fusion = (bf16[2,128,512]{2,1,0:T(8,128)(2,1)}, bf16[2,128,512]{2,1,0:T(8,128)(2,1)}) fusion(bf16[128,2,512]{2,1,0:T(2,128)(2,1)} %param.22, bf16[128,2,512]{2,1,0:T(2,128)(2,1)} %param.21), kind=kLoop, calls=%fused_computation.5 | loop fusion | bytes 1048576 | tf_op jit(solution)/shard_map/transpose | solution.py:732
  6.5 0.8 copy.19
  7.3 0.2 reduce_window_sum.11.cumul_ref
  7.4 0.0 copy-start
  7.4 0.7 copy.20
  8.1 0.0 copy-done
  8.1 0.0 copy-start.1
  8.1 0.0 copy-start.2
  8.1 168.1 %shard_map.154 = (bf16[512,1024]{1,0:T(8,128)(2,1)}, f32[128,1024]{1,0:T(8,128)}) custom-call(bf16[128,1024]{1,0:T(8,128)(2,1)} %residual_ref.1, bf16[128,512]{1,0:T(8,128)(2,1)} %query_a_ref.1, bf16[128,512]{1,0:T(8,128)(2,1)} %key_a_ref.1, bf16[128,1024]{1,0:T(8,128)(2,1)} %query_b_ref.1, bf16[128,1024]{1,0:T(8,128)(2,1)} %key_b_ref.1, ...), custom_call_target="tpu_custom_call" | custom-call | tf_op jit(solution)/shard_map/pallas_call | solution.py:668
  176.2 0.0 copy-done.1
  176.2 0.0 copy-done.2
  176.2 1.6 convolution_multiply_fusion.1
  177.8 2.4 %fusion.2 = bf16[128,1024]{1,0:T(8,128)(2,1)} fusion(f32[128,1024]{1,0:T(8,128)} %get-tuple-element.7, f32[128,1024]{1,0:T(8,128)S(1)} %convolution_multiply_fusion.1, bf16[512,1024]{1,0:T(8,128)(2,1)} %get-tuple-element.8, f32[128]{0:T(128)S(1)} %get-tuple-element.15, s32[128]{0:T(128)S(1)} %get-tuple-element.13), kind=kOutput, calls=%fused_computation.4 | convolution fusion | flops 134807552 | bytes 2360320 | tf_op jit(solution)/shard_map/dot_general | solution.py:749
  (6 shorter events, 0.0 us)
Async XLA Ops:
  7.4 0.7 copy-start
  8.1 168.1 %copy-start.1 = (s32[128,2]{0,1:T(2,128)S(1)}, s32[128,2]{0,1:T(2,128)}, u32[]{:S(2)}) copy-start(s32[128,2]{0,1:T(2,128)} %param.27) | copy-start | bytes 3076
  8.1 168.1 %copy-start.2 = (f32[128,2]{0,1:T(2,128)S(1)}, f32[128,2]{0,1:T(2,128)}, u32[]{:S(2)}) copy-start(f32[128,2]{0,1:T(2,128)} %param.28) | copy-start | bytes 3076

commit v3 on v2

--- a/solution.py
+++ b/solution.py
@@ -1,5 +1,6 @@
 import jax
 import jax.numpy as jnp
+import numpy as np
 from jax import lax
 from jax.experimental import pallas as pl
 from jax.experimental.pallas import tpu as pltpu
@@ -40,7 +41,7 @@
     )
 
 
-GROUPS = 4
+GROUPS = 8
 
 
 def grid_of(count):
@@ -48,9 +49,12 @@
     return across, count // across
 
 
-def group_order():
-    middle = (GROUPS - 1) / 2
-    return sorted(range(GROUPS), key=lambda g: (abs(g - middle), g))
+QUARTERS = ((0, 2, 3, 1), (1, 2, 0, 3), (2, 1, 3, 0), (3, 1, 0, 2))
+SENDS = ((1, 3, 2), (2, 3, 0), (1, 0, 3), (2, 0, 1))
+ORDER = tuple(
+    (k,) + tuple(2 * q + i for q in QUARTERS[k // 2][1:] for i in range(2)) + (k ^ 1,)
+    for k in range(GROUPS)
+)
 
 
 def turned(block, cosine, sine):
@@ -70,21 +74,23 @@
     key_b_ref,
     values_ref,
     gates_ref,
-    cos_a_ref,
-    sin_a_ref,
-    cos_b_ref,
-    sin_b_ref,
-    cumul_ref,
-    cumul_rows_ref,
+    turn_a_ref,
+    start_a_ref,
+    turn_b_ref,
+    start_b_ref,
+    decay_ref,
     head_gain_ref,
     gain_ref,
-    target_ref,
+    routes_ref,
+    route_weight_ref,
     weight_hbm,
     gate_hbm,
     up_hbm,
     down_hbm,
     out_ref,
     stream_ref,
+    cumul_ref,
+    cumul_rows_ref,
     rot_queries_a,
     rot_queries_b,
     within,
@@ -102,6 +108,9 @@
     outgoing,
     arrived,
     hidden,
+    far_heads,
+    far_out,
+    far_in,
     result,
     returned,
     acc_a,
@@ -115,6 +124,8 @@
     w_line_send,
     w_pair_send,
     w_recv,
+    far_send,
+    far_recv,
     sq_send,
     sq_recv,
     disp_send,
@@ -134,7 +145,6 @@
     s, t = lax.axis_index("sp"), lax.axis_index("tp")
     bf16, f32 = jnp.bfloat16, jnp.float32
     per_group = n_sp // GROUPS
-    order = group_order()
     across, down = grid_of(n_tp)
     x, y = t % across, t // across
     cap = outgoing.shape[0] // n_sp
@@ -153,7 +163,8 @@
     own_load.start()
     for load in loads:
         load.start()
-    greet(("sp", "tp"))
+    with jax.named_scope("greet"):
+        greet(("sp", "tp"))
 
     partner = s + 1 - 2 * core
     ahead = s + 2 - 4 * core
@@ -165,14 +176,17 @@
     def to_partner(b):
         return remote(w_out.at[b], w_out.at[b], w_pair_send.at[b], w_recv.at[b], "sp", partner)
 
-    def pass_on(b):
-        @pl.when(has_ahead)
+    reach = chips - 2
+
+    def pass_on(b, j):
+        @pl.when(has_ahead & (j < reach))
         def _():
             along_line(b).start()
 
-    own_load.wait()
+    with jax.named_scope("own"):
+        own_load.wait()
     to_partner(s).start()
-    pass_on(s)
+    pass_on(s, 0)
 
     def chip_behind(j):
         return z + (2 * core - 1) * j
@@ -185,18 +199,32 @@
             b = chip * 2 + i
             along_line(b).wait_recv()
             to_partner(b).start()
-            pass_on(b)
-
-    head_count = cumul_ref.shape[1] // 2
+            pass_on(b, j)
+
+    head_count = decay_ref.shape[0] // 2
     groups = (
-        (query_a_ref, key_a_ref, cos_a_ref, sin_a_ref, rot_queries_a),
-        (query_b_ref, key_b_ref, cos_b_ref, sin_b_ref, rot_queries_b),
+        (query_a_ref, key_a_ref, turn_a_ref, start_a_ref, rot_queries_a),
+        (query_b_ref, key_b_ref, turn_b_ref, start_b_ref, rot_queries_b),
     )
     size_a = query_a_ref.shape[1] // head_count
     dv = values_ref.shape[2] // head_count
     rows_i = lax.broadcasted_iota(jnp.int32, (count, count), 0)
     rows_j = lax.broadcasted_iota(jnp.int32, (count, count), 1)
     causal = rows_i >= rows_j
+    exact = lax.Precision.HIGHEST
+    cumul_rows_ref[...] = jnp.dot(
+        decay_ref[...],
+        jnp.where(rows_i <= rows_j, 1.0, 0.0),
+        precision=exact,
+        preferred_element_type=f32,
+    )
+    cumul_ref[...] = lax.dot_general(
+        jnp.where(causal, 1.0, 0.0),
+        decay_ref[...],
+        (((1,), (1,)), ((), ())),
+        precision=exact,
+        preferred_element_type=f32,
+    )
 
     def hop(c):
         return remote(
@@ -205,12 +233,14 @@
 
     pieces_of = []
     total_pieces = 0
-    for g, (query_ref, key_ref, cos_ref, sin_ref, rot_ref) in enumerate(groups):
+    for g, (query_ref, key_ref, turn_ref, start_ref, rot_ref) in enumerate(groups):
         size = query_ref.shape[1] // head_count
+        cos_start, sin_start = start_ref[0, pl.ds(s, 1), :], start_ref[1, pl.ds(s, 1), :]
+        cosine = cos_start * turn_ref[0] - sin_start * turn_ref[1]
+        sine = sin_start * turn_ref[0] + cos_start * turn_ref[1]
         for h in range(head_count):
             i = g * head_count + h
             lanes = slice(h * size, (h + 1) * size)
-            cosine, sine = cos_ref[...], sin_ref[...]
             rot_q = turned(query_ref[:, lanes].astype(f32), cosine, sine).astype(bf16)
             rot_k = (turned(key_ref[:, lanes].astype(f32), cosine, sine) * size ** (-0.5)).astype(
                 bf16
@@ -222,7 +252,7 @@
             )
             spread = column - row
             weight = jnp.where(causal, jnp.exp(jnp.where(causal, spread, 0.0)), 0.0)
-            value = values_ref[g, :, h * dv : (h + 1) * dv]
+            value = values_ref[:, g, h * dv : (h + 1) * dv]
             within[i] = jnp.dot(
                 (scores * weight).astype(bf16), value, preferred_element_type=f32
             )
@@ -240,8 +270,9 @@
             pieces_of.append(mine)
 
     to_line = partner
-    to_partner(partner).wait_recv()
-    pass_on(to_line)
+    with jax.named_scope("pair"):
+        to_partner(partner).wait_recv()
+    pass_on(to_line, 0)
 
     def step(c, _):
         @pl.when(s == 0)
@@ -259,9 +290,11 @@
 
         return 0
 
-    lax.fori_loop(0, total_pieces, step, 0)
-
-    serve(1, 0)
+    with jax.named_scope("chain"):
+        lax.fori_loop(0, total_pieces, step, 0)
+
+    with jax.named_scope("serve0"):
+        serve(1, 0)
 
     def heads_copy(g, k, source):
         block = heads.at[source, g]
@@ -283,7 +316,7 @@
                 jnp.mean(retained * retained, axis=1, keepdims=True) + EPS
             )
             lanes = slice(h * dv, (h + 1) * dv)
-            gated = jax.nn.silu(gates_ref[g, :, lanes].astype(f32))
+            gated = jax.nn.silu(gates_ref[:, g, lanes].astype(f32))
             heads[t, g, :, lanes] = (scaled * head_gain_ref[g : g + 1, lanes] * gated).astype(bf16)
 
         def heads_start(k, _, g=g):
@@ -292,14 +325,35 @@
 
         lax.fori_loop(1, n_tp, heads_start, 0)
 
-    serve(1, 1)
+    with jax.named_scope("serve1"):
+        serve(1, 1)
     for g in range(2):
 
         def heads_wait(k, _, g=g):
             heads_copy(g, k, (t + k) % n_tp).wait_recv()
             return 0
 
-        lax.fori_loop(1, n_tp, heads_wait, 0)
+        with jax.named_scope("headswait"):
+            lax.fori_loop(1, n_tp, heads_wait, 0)
+
+    at_low, at_high = z == 0, z == chips - 1
+    near_low, near_high = z == 1, z == chips - 2
+
+    def far_pair(low, shift, action):
+        @pl.when(low)
+        def _():
+            action(shift)
+
+    def ask(shift):
+        return remote(
+            heads.at[chips - 1 - z], far_heads, far_send.at[0], far_recv.at[0], "sp", s + shift
+        )
+
+    def answer(shift):
+        return remote(far_out, far_in, far_send.at[1], far_recv.at[1], "sp", s + shift)
+
+    far_pair(at_low, 2, lambda shift: ask(shift).start())
+    far_pair(at_high, -2, lambda shift: ask(shift).start())
 
     held_rows = w_out.shape[2]
     ratio = n_sp // n_tp
@@ -348,15 +402,40 @@
         project_chips(j, False)
         return 0
 
+    def project_edge(shift):
+        ask(shift).wait_recv()
+        far = chips - 1 if shift < 0 else 0
+        part = jnp.zeros((count, cols), f32)
+        for i in range(2):
+            lanes = slice(i * held_rows, (i + 1) * held_rows)
+            for g in range(2):
+                part += jnp.dot(
+                    far_heads[g, :, lanes], w_out[2 * far + i, g], preferred_element_type=f32
+                )
+        far_out[...] = part.astype(bf16)
+        answer(shift).start()
+
+    def add_edge(shift):
+        answer(shift).wait_recv()
+        mix[...] += far_in[...].astype(f32)
+
     def rows_of(p):
         return pl.ds(pl.multiple_of(p * cap, cap), cap)
 
+    eighth, quarter = s // per_group, s // (n_sp // 4)
+
+    def group_base(g):
+        base = ORDER[0][g]
+        for k in range(1, GROUPS):
+            base = jnp.where(eighth == k, ORDER[k][g], base)
+        return base * per_group
+
     def group_rows(g, part=None):
         size = per_group * cap
-        start = order[g] * size
+        start = pl.multiple_of(group_base(g) * cap, size)
         if part is None:
             return pl.ds(start, size)
-        return pl.ds(start + part * (size // 2), size // 2)
+        return pl.ds(pl.multiple_of(start + part * (size // 2), size // 2), size // 2)
 
     def square_copy(k, source):
         block, other = squares.at[source], (t + k) % n_tp
@@ -374,7 +453,7 @@
 
     def members(g, action):
         def body(j, _):
-            action(order[g] * per_group + j)
+            action(group_base(g) + j)
             return 0
 
         lax.fori_loop(0, per_group, body, 0)
@@ -386,6 +465,17 @@
                 action(p)
 
         members(g, guarded)
+
+    def choice(c):
+        numbers = lax.broadcasted_iota(jnp.int32, (n_sp, count), 0)
+        named = [numbers == routes_ref[k : k + 1, :] for k in range(2)]
+        counted = [jnp.where(mask, 1.0, 0.0).astype(bf16) for mask in named]
+        earlier = jnp.where(rows_i < rows_j, 1.0, 0.0).astype(bf16)
+        before = jnp.dot(counted[0] + counted[1], earlier, preferred_element_type=f32)
+        slot = jnp.sum(jnp.where(named[c], before, 0.0), axis=0, keepdims=True)
+        target = routes_ref[c : c + 1, :] * cap + slot.astype(jnp.int32)
+        slots = lax.broadcasted_iota(jnp.int32, (outgoing.shape[0], count), 0)
+        return jnp.where(slots == target, 1.0, 0.0).astype(bf16)
 
     def finish_rows():
         stream = residual_ref[...].astype(f32) + mix[...].astype(bf16).astype(f32)
@@ -409,13 +499,28 @@
         scale = lax.rsqrt(total[0:1, :] / (cols * n_tp) + EPS)
         scale = jnp.broadcast_to(scale, (count, count)).T[:, 0:1]
         normed = (stream_ref[...] * scale * gain_ref[...]).astype(bf16)
-        slots = lax.broadcasted_iota(jnp.int32, (outgoing.shape[0], count), 0)
-        select = (slots == target_ref[0:1, :]) | (slots == target_ref[1:2, :])
-        select = jnp.where(select, 1.0, 0.0).astype(bf16)
+        select = choice(0) + choice(1)
         outgoing[...] = jnp.dot(select, normed, preferred_element_type=f32).astype(bf16)
-        for g in range(GROUPS):
-            others(g, lambda p: dispatch(p, s).start())
         arrived[t, rows_of(s)] = outgoing[rows_of(s)]
+
+    def dispatch_to(q):
+        def body(j, _):
+            p = q * (n_sp // 4) + j
+
+            @pl.when(p != s)
+            def _():
+                dispatch(p, s).start()
+
+            return 0
+
+        lax.fori_loop(0, n_sp // 4, body, 0)
+
+    def dispatch_stage(i):
+        for q in range(4):
+
+            @pl.when(quarter == q)
+            def _(q=q):
+                dispatch_to(SENDS[q][i])
 
     lines = (
         [y * across + (x + k) % across for k in range(1, across)],
@@ -472,7 +577,8 @@
             for i in range(len(direct)):
                 straight(arrived, arrived_sems, g, i, t, rows_of(p)).start()
 
-        members(g, block)
+        with jax.named_scope("forward"):
+            members(g, block)
 
     def through_units(g):
         acc_a[...] = jnp.zeros_like(acc_a)
@@ -487,7 +593,8 @@
             acc_b[...] += jnp.dot(rows, w_up[part, :], preferred_element_type=f32)
             return 0
 
-        lax.fori_loop(0, n_tp, body, 0)
+        with jax.named_scope("units"):
+            lax.fori_loop(0, n_tp, body, 0)
         hidden[t, group_rows(g)] = (jax.nn.silu(acc_a[...]) * acc_b[...]).astype(bf16)
         for i in range(len(direct)):
             straight(hidden, hidden_sems, g, i, t, group_rows(g)).start()
@@ -509,58 +616,55 @@
             )
             return 0
 
-        lax.fori_loop(0, n_tp, body, 0)
+        with jax.named_scope("down"):
+            lax.fori_loop(0, n_tp, body, 0)
         result[group_rows(g)] = acc_c[...].astype(bf16)
         others(g, lambda p: give_back(p, s).start())
 
-    relay_rows = lambda g: relay(arrived, arrived_sems, g)
-    relay_hidden = lambda g: relay(hidden, hidden_sems, g)
-
-    inner_lo, inner_hi = chips // 4, chips - chips // 4
-    inner = (z >= inner_lo) & (z < inner_hi)
-    if chips > 1:
+    def relay_rows(g):
+        with jax.named_scope("relay_rows"):
+            relay(arrived, arrived_sems, g)
+
+    def relay_hidden(g):
+        with jax.named_scope("relay_hidden"):
+            relay(hidden, hidden_sems, g)
+
+    with jax.named_scope("proj1"):
         project_chips(1, True)
-    lax.fori_loop(2, inner_hi, project_far, 0)
-
-    @pl.when(inner)
-    def _():
+    with jax.named_scope("proj2"):
+        lax.fori_loop(2, reach + 1, project_far, 0)
+    far_pair(near_low, -2, project_edge)
+    far_pair(near_high, 2, project_edge)
+    with jax.named_scope("edge"):
+        far_pair(at_low, 2, add_edge)
+        far_pair(at_high, -2, add_edge)
+    with jax.named_scope("finish"):
         finish_rows()
-
-    half = GROUPS // 2
-    for g in range(half):
-        forward(g)
-    for g in range(half):
-        relay_rows(g)
+    dispatch_stage(0)
+    dispatch_to(quarter)
     for load in loads:
         load.wait()
-    for g in range(half):
-        through_units(g)
-
-    lax.fori_loop(inner_hi, chips, project_far, 0)
-
-    @pl.when(jnp.logical_not(inner))
-    def _():
-        finish_rows()
-
-    for g in range(half):
-        relay_hidden(g)
-    for g in range(half):
-        through_down(g)
-    for g in range(half, GROUPS):
-        forward(g)
-    for g in range(half, GROUPS):
-        relay_rows(g)
-    for g in range(half, GROUPS):
-        through_units(g)
-    for g in range(half, GROUPS):
-        relay_hidden(g)
-    for g in range(half, GROUPS):
-        through_down(g)
+    for step in range(GROUPS + 4):
+        for late, action in enumerate(
+            (forward, relay_rows, through_units, relay_hidden, through_down)
+        ):
+            if 0 <= step - late < GROUPS:
+                action(step - late)
+            if late == 1 and step in (1, 3):
+                dispatch_stage((step + 1) // 2)
 
     returned[rows_of(s)] = result[rows_of(s)]
-    for g in range(GROUPS):
-        others(g, lambda p: give_back(p, p).wait_recv())
-    out_ref[...] = returned[...]
+    with jax.named_scope("back"):
+        for g in range(GROUPS):
+            others(g, lambda p: give_back(p, p).wait_recv())
+    total = stream_ref[...]
+    for c in range(2):
+        pick = lax.dot_general(
+            choice(c), returned[...], (((0,), (0,)), ((), ())), preferred_element_type=f32
+        )
+        share = jnp.broadcast_to(route_weight_ref[c : c + 1, :], (count, count)).T[:, 0:1]
+        total = total + share * pick
+    out_ref[...] = total.astype(bf16)
 
     @pl.when(s < n_sp - 1)
     def _():
@@ -586,7 +690,7 @@
             for i in range(2):
                 b = chip * 2 + i
 
-                @pl.when(has_ahead)
+                @pl.when(has_ahead & (j < reach))
                 def _():
                     along_line(b).wait_send()
 
@@ -596,7 +700,11 @@
 
         return 0
 
-    lax.fori_loop(0, chips, passed, 0)
+    lax.fori_loop(0, reach + 1, passed, 0)
+    far_pair(at_low, 2, lambda shift: ask(shift).wait_send())
+    far_pair(at_high, -2, lambda shift: ask(shift).wait_send())
+    far_pair(near_low, -2, lambda shift: answer(shift).wait_send())
+    far_pair(near_high, 2, lambda shift: answer(shift).wait_send())
     for g in range(GROUPS):
         others(g, lambda p: dispatch(p, s).wait_send())
         others(g, lambda p: give_back(p, s).wait_send())
@@ -604,13 +712,17 @@
         finish_sends(hidden, hidden_sems, g)
 
 
-def tables(positions, size):
+def tables(rows, blocks, size):
     half = size // 2
-    inverse = jnp.power(THETA, -jnp.arange(half, dtype=jnp.float32) * 2.0 / size)
-    inverse = jnp.concatenate([inverse, inverse])
-    sign = jnp.where(jnp.arange(size) < half, -1.0, 1.0)
-    angles = positions[:, None] * inverse[None, :]
-    return jnp.cos(angles), jnp.sin(angles) * sign[None, :]
+    inverse = np.power(THETA, -np.arange(half) * 2.0 / size)
+    inverse = np.concatenate([inverse, inverse])
+    sign = np.where(np.arange(size) < half, -1.0, 1.0)
+
+    def at(positions):
+        angles = positions[:, None] * inverse[None, :]
+        return jnp.asarray(np.stack([np.cos(angles), np.sin(angles) * sign]), jnp.float32)
+
+    return at(np.arange(rows)), at(np.arange(blocks) * rows)
 
 
 def per_device(
@@ -635,28 +747,10 @@
     row_count, cols = residual.shape
     head_count = log_decay.shape[2]
     bf16, f32 = jnp.bfloat16, jnp.float32
-    positions = (lax.axis_index("sp") * row_count + jnp.arange(row_count, dtype=jnp.int32)).astype(
-        f32
-    )
     size_a, size_b = query_small.shape[1] // head_count, query_large.shape[1] // head_count
-    cos_a, sin_a = tables(positions, size_a)
-    cos_b, sin_b = tables(positions, size_b)
-    cumul = jnp.cumsum(log_decay.reshape(row_count, 2 * head_count), axis=0)
-
-    experts = n_sp
-    capacity = 4 * row_count // experts
-    slots = experts * capacity
-    numbers = jnp.arange(experts, dtype=jnp.int32)
-    named = [(routes[:, c][:, None] == numbers[None, :]) for c in range(2)]
-    counted = (named[0].astype(bf16) + named[1].astype(bf16))
-    earlier = jnp.arange(row_count)[:, None] > jnp.arange(row_count)[None, :]
-    before = jnp.dot(earlier.astype(bf16), counted, preferred_element_type=f32)
-    target = [
-        routes[:, c] * capacity
-        + jnp.sum(jnp.where(named[c], before, 0.0), axis=1).astype(jnp.int32)
-        for c in range(2)
-    ]
-
+    turn_a, start_a = tables(row_count, n_sp, size_a)
+    turn_b, start_b = tables(row_count, n_sp, size_b)
+    slots = 4 * row_count
     pieces = head_count * (1 + size_b // size_a)
     value_size = values.shape[2] // head_count
     width, units = expert_gate.shape[1:]
@@ -665,15 +759,15 @@
     straights, relays = across + down - 2, (across - 1) * (down - 1)
     vmem = pl.BlockSpec(memory_space=pltpu.VMEM)
     hbm = pl.BlockSpec(memory_space=pl.ANY)
-    returned, stream = pl.pallas_call(
+    return pl.pallas_call(
         layer_kernel,
-        out_shape=(
-            jax.ShapeDtypeStruct((slots, cols), bf16),
-            jax.ShapeDtypeStruct((row_count, cols), f32),
-        ),
+        out_shape=jax.ShapeDtypeStruct((row_count, cols), bf16),
         in_specs=[vmem] * 16 + [hbm] * 4,
-        out_specs=(vmem, vmem),
+        out_specs=vmem,
         scratch_shapes=[
+            pltpu.VMEM((row_count, cols), f32),
+            pltpu.VMEM((row_count, 2 * head_count), f32),
+            pltpu.VMEM((2 * head_count, row_count), f32),
             pltpu.VMEM(query_small.shape, bf16),
             pltpu.VMEM(query_large.shape, bf16),
             pltpu.VMEM((2 * head_count, row_count, value_size), f32),
@@ -691,6 +785,9 @@
             pltpu.VMEM((slots, cols), bf16),
             pltpu.VMEM((n_tp, slots, cols), bf16),
             pltpu.VMEM((n_tp, slots, units), bf16),
+            pltpu.VMEM((2, row_count, values.shape[2]), bf16),
+            pltpu.VMEM((row_count, cols), bf16),
+            pltpu.VMEM((row_count, cols), bf16),
             pltpu.VMEM((slots, cols), bf16),
             pltpu.VMEM((slots, cols), bf16),
             pltpu.VMEM((slots // GROUPS, units), f32),
@@ -704,6 +801,8 @@
             dma((n_sp,)),
             dma((n_sp,)),
             dma((n_sp,)),
+            dma((2,)),
+            dma((2,)),
             dma((n_tp,)),
             dma((n_tp,)),
             dma((n_sp,)),
@@ -728,31 +827,22 @@
         key_narrow_group,
         query_large,
         key_large,
-        jnp.swapaxes(values, 0, 1),
-        jnp.swapaxes(gates, 0, 1),
-        cos_a,
-        sin_a,
-        cos_b,
-        sin_b,
-        cumul,
-        cumul.T,
+        values,
+        gates,
+        turn_a,
+        start_a,
+        turn_b,
+        start_b,
+        jnp.transpose(log_decay, (1, 2, 0)).reshape(2 * head_count, row_count),
         head_gain,
         norm_gain[None, :],
-        jnp.stack(target),
+        routes.T,
+        route_weight.T,
         out_weight,
         expert_gate,
         expert_up,
         expert_down,
     )
-    ids = jnp.arange(slots, dtype=jnp.int32)[None, :]
-    picks = [
-        jnp.dot(
-            (target[c][:, None] == ids).astype(bf16), returned, preferred_element_type=f32
-        )
-        for c in range(2)
-    ]
-    routed = route_weight[:, 0:1] * picks[0] + route_weight[:, 1:2] * picks[1]
-    return (stream + routed).astype(bf16)
 
 
 def solution(mesh):

time: 180 us -> 136 us (0.76)
  Pallas kernels: 168 us -> 133 us
  matrix products: 4.13 us -> 0 us
  other arithmetic: 3.86 us -> 0 us
  local copies, waits for them, and re-layouts: 4.09 us -> 1.67 us
    pallas_call x1, Pallas kernels: 168 us -> 133 us  [per_device(): pl.pallas_call(layer_kernel, out_shape=jax.ShapeDtypeStruct((row_count, c...]
    dot_general x3 -> x0, matrix products: 4.13 us -> none  [the longest x2 3.98 us: per_device(): jnp.dot((target[c][:, None] == ids).astype(bf16), returned, preferred_ele...]
    mul x2 -> x0, other arithmetic: 2.22 us -> none  [tables(): return (jnp.cos(angles), jnp.sin(angles) * sign[None, :])]
    transpose x1 -> x0, local copies, waits for them, and re-layouts: 1.87 us -> none  [per_device(): jnp.swapaxes(gates, 0, 1)]
where the time goes in v3:
time: 136 us; the launch traced here: 134 us
  Pallas kernels  133 us (98%)
  local copies, waits for them, and re-layouts  1.67 us (1%)
    pallas_call x1, Pallas kernels, per_device(): pl.pallas_call(layer_kernel, out_shape=jax.ShapeDtypeStruct((row_count, c...  133 us

profile of v3, /device:TPU:1, one launch (start us, length us, event | category | flops | bytes accessed | tf_op | source)
XLA Modules:
  0.0 134.5 jit_solution(12673096484291064138)
XLA Ops:
  0.0 132.8 %shard_map.190 = bf16[128,1024]{1,0:T(8,128)(2,1)} custom-call(bf16[128,1024]{1,0:T(8,128)(2,1)} %residual_ref.1, bf16[128,512]{1,0:T(8,128)(2,1)} %query_a_ref.1, bf16[128,512]{1,0:T(8,128)(2,1)} %key_a_ref.1, bf16[128,1024]{1,0:T(8,128)(2,1)} %query_b_ref.1, bf16[128,1024]{1,0:T(8,128)(2,1)} %key_b_ref.1, bf16[128,2,512]{2,1,0:T(2,128)(2,1)} %values_ref.1, ...), custom_call_target="tpu_custom_call" | custom-call | tf_op jit(solution)/shard_map/pallas_call | solution.py:762
  132.8 1.7 %copy.22 = bf16[128,1024]{1,0:T(8,128)(2,1)} copy(bf16[128,1024]{1,0:T(8,128)(2,1)} %shard_map.190) | data formatting | bytes 524288

commit v4 on v3

--- a/solution.py
+++ b/solution.py
@@ -49,11 +49,17 @@
     return across, count // across
 
 
-QUARTERS = ((0, 2, 3, 1), (1, 2, 0, 3), (2, 1, 3, 0), (3, 1, 0, 2))
-SENDS = ((1, 3, 2), (2, 3, 0), (1, 0, 3), (2, 0, 1))
-ORDER = tuple(
-    (k,) + tuple(2 * q + i for q in QUARTERS[k // 2][1:] for i in range(2)) + (k ^ 1,)
-    for k in range(GROUPS)
+BETWEEN = ((2, 4, 5, 6, 7, 3), (4, 0, 1, 6, 7, 5), (2, 6, 7, 0, 1, 3), (4, 2, 3, 0, 1, 5))
+ORDER = tuple((k,) + BETWEEN[k // 2] + (k ^ 1,) for k in range(GROUPS))
+SENDS = (
+    ((1, -2), (2, 3), (3, 4)),
+    ((1, -2), (2, 3), (3, 4)),
+    ((0, -2), (2, -2), (3, 2)),
+    ((3, 3), (0, 4), (2, 5)),
+    ((1, -2), (3, -1), (0, -1)),
+    ((0, -1), (1, 4), (3, 5)),
+    ((2, -2), (1, -1), (0, 2)),
+    ((2, -2), (1, -1), (0, 2)),
 )
 
 
@@ -66,7 +72,22 @@
     return block * cosine + swapped * sine
 
 
-def layer_kernel(
+STAGED = 16
+
+
+def layer_kernel(*refs):
+    sources, refs = refs[:STAGED], refs[STAGED:]
+    weights_and_out, refs = refs[:5], refs[5:]
+    places, load_sem, refs = refs[:STAGED], refs[STAGED], refs[STAGED + 1 :]
+    staged = [
+        pltpu.make_async_copy(source, place, load_sem.at[i])
+        for i, (source, place) in enumerate(zip(sources, places, strict=True))
+    ]
+    layer(staged, *places, *weights_and_out, *refs)
+
+
+def layer(
+    staged,
     residual_ref,
     query_a_ref,
     key_a_ref,
@@ -88,6 +109,9 @@
     up_hbm,
     down_hbm,
     out_ref,
+    picks,
+    select,
+    shares,
     stream_ref,
     cumul_ref,
     cumul_rows_ref,
@@ -108,6 +132,8 @@
     outgoing,
     arrived,
     hidden,
+    scales_out,
+    scales,
     far_heads,
     far_out,
     far_in,
@@ -130,6 +156,8 @@
     sq_recv,
     disp_send,
     disp_recv,
+    scale_send,
+    scale_recv,
     fwd_send,
     fwd_recv,
     fwd_relay_send,
@@ -161,6 +189,8 @@
     ]
     own_load = pltpu.make_async_copy(weight_hbm, w_out.at[s], load_sem.at[3])
     own_load.start()
+    for load in staged:
+        load.start()
     for load in loads:
         load.start()
     with jax.named_scope("greet"):
@@ -170,36 +200,58 @@
     ahead = s + 2 - 4 * core
     has_ahead = jnp.where(core == 0, z < chips - 1, z > 0)
 
-    def along_line(b):
-        return remote(w_out.at[b], w_out.at[b], w_line_send.at[b], w_recv.at[b], "sp", ahead)
-
-    def to_partner(b):
-        return remote(w_out.at[b], w_out.at[b], w_pair_send.at[b], w_recv.at[b], "sp", partner)
+    wide = cols // 2
+
+    def half(h):
+        return pl.ds(h * wide, wide)
+
+    def along_line(b, h):
+        block = w_out.at[b, :, :, half(h)]
+        return remote(block, block, w_line_send.at[h, b], w_recv.at[h, b], "sp", ahead)
+
+    def to_partner(b, h):
+        block = w_out.at[b, :, :, half(h)]
+        return remote(block, block, w_pair_send.at[h, b], w_recv.at[h, b], "sp", partner)
 
     reach = chips - 2
 
-    def pass_on(b, j):
+    def pass_on(b, h, j):
         @pl.when(has_ahead & (j < reach))
         def _():
-            along_line(b).start()
+            along_line(b, h).start()
 
     with jax.named_scope("own"):
         own_load.wait()
-    to_partner(s).start()
-    pass_on(s, 0)
+    for h in range(2):
+        to_partner(s, h).start()
+        pass_on(s, h, 0)
+    for load in staged:
+        load.wait()
 
     def chip_behind(j):
         return z + (2 * core - 1) * j
 
-    def serve(j, i):
+    def serve(j, h, i):
         chip = chip_behind(j)
 
         @pl.when((chip >= 0) & (chip < chips))
         def _():
             b = chip * 2 + i
-            along_line(b).wait_recv()
-            to_partner(b).start()
-            pass_on(b, j)
+            along_line(b, h).wait_recv()
+            to_partner(b, h).start()
+            if h == 0:
+                pass_on(b, h, j)
+
+    def serve_right(j):
+        for i in range(2):
+            serve(j, 1, i)
+        chip = chip_behind(j)
+
+        @pl.when((chip >= 0) & (chip < chips) & has_ahead & (j < reach))
+        def _():
+            for i in range(2):
+                along_line(chip * 2 + i, 0).wait_send()
+                along_line(chip * 2 + i, 1).start()
 
     head_count = decay_ref.shape[0] // 2
     groups = (
@@ -269,10 +321,9 @@
                 total_pieces += 1
             pieces_of.append(mine)
 
-    to_line = partner
-    with jax.named_scope("pair"):
-        to_partner(partner).wait_recv()
-    pass_on(to_line, 0)
+    for h in range(2):
+        to_partner(partner, h).wait_recv()
+        pass_on(partner, h, 0)
 
     def step(c, _):
         @pl.when(s == 0)
@@ -294,7 +345,7 @@
         lax.fori_loop(0, total_pieces, step, 0)
 
     with jax.named_scope("serve0"):
-        serve(1, 0)
+        serve(1, 0, 0)
 
     def heads_copy(g, k, source):
         block = heads.at[source, g]
@@ -326,7 +377,7 @@
         lax.fori_loop(1, n_tp, heads_start, 0)
 
     with jax.named_scope("serve1"):
-        serve(1, 1)
+        serve(1, 0, 1)
     for g in range(2):
 
         def heads_wait(k, _, g=g):
@@ -349,8 +400,15 @@
             heads.at[chips - 1 - z], far_heads, far_send.at[0], far_recv.at[0], "sp", s + shift
         )
 
-    def answer(shift):
-        return remote(far_out, far_in, far_send.at[1], far_recv.at[1], "sp", s + shift)
+    def answer(shift, h):
+        return remote(
+            far_out.at[:, half(h)],
+            far_in.at[:, half(h)],
+            far_send.at[1 + h],
+            far_recv.at[1 + h],
+            "sp",
+            s + shift,
+        )
 
     far_pair(at_low, 2, lambda shift: ask(shift).start())
     far_pair(at_high, -2, lambda shift: ask(shift).start())
@@ -358,65 +416,60 @@
     held_rows = w_out.shape[2]
     ratio = n_sp // n_tp
 
-    def project_lanes(b, lanes):
-        part = jnp.dot(heads[b // ratio, 0, :, lanes], w_out[b, 0], preferred_element_type=f32)
-        part += jnp.dot(heads[b // ratio, 1, :, lanes], w_out[b, 1], preferred_element_type=f32)
-        mix[...] += part
-
-    def project(b):
+    def project_lanes(b, h, lanes):
+        part = jnp.dot(
+            heads[b // ratio, 0, :, lanes], w_out[b, 0, :, half(h)], preferred_element_type=f32
+        )
+        part += jnp.dot(
+            heads[b // ratio, 1, :, lanes], w_out[b, 1, :, half(h)], preferred_element_type=f32
+        )
+        mix[:, half(h)] += part
+
+    def project(b, h):
         if held_rows % 128 == 0:
             project_lanes(
-                b, pl.ds(pl.multiple_of((b % ratio) * held_rows, held_rows), held_rows)
+                b, h, pl.ds(pl.multiple_of((b % ratio) * held_rows, held_rows), held_rows)
             )
             return
         for r in range(ratio):
 
             @pl.when(b % ratio == r)
             def _(r=r):
-                project_lanes(b, slice(r * held_rows, (r + 1) * held_rows))
-
-    mix[...] = jnp.zeros_like(mix)
-    for i in range(2):
-        project(z * 2 + i)
-
-    def project_chips(j, served):
-        for i in range(2):
-            if not served:
-                serve(j, i)
+                project_lanes(b, h, slice(r * held_rows, (r + 1) * held_rows))
+
+    def project_chips(j, h):
         chip = chip_behind(j)
 
         @pl.when((chip >= 0) & (chip < chips))
         def _():
             for i in range(2):
-                project(chip * 2 + i)
+                project(chip * 2 + i, h)
 
         other = z - (2 * core - 1) * j
 
         @pl.when((other >= 0) & (other < chips))
         def _():
             for i in range(2):
-                to_partner(other * 2 + i).wait_recv()
-                project(other * 2 + i)
-
-    def project_far(j, _):
-        project_chips(j, False)
-        return 0
-
-    def project_edge(shift):
-        ask(shift).wait_recv()
+                to_partner(other * 2 + i, h).wait_recv()
+                project(other * 2 + i, h)
+
+    def project_edge(shift, h):
         far = chips - 1 if shift < 0 else 0
-        part = jnp.zeros((count, cols), f32)
+        part = jnp.zeros((count, wide), f32)
         for i in range(2):
             lanes = slice(i * held_rows, (i + 1) * held_rows)
             for g in range(2):
                 part += jnp.dot(
-                    far_heads[g, :, lanes], w_out[2 * far + i, g], preferred_element_type=f32
+                    far_heads[g, :, lanes],
+                    w_out[2 * far + i, g, :, half(h)],
+                    preferred_element_type=f32,
                 )
-        far_out[...] = part.astype(bf16)
-        answer(shift).start()
+        far_out[:, half(h)] = part.astype(bf16)
+        answer(shift, h).start()
 
     def add_edge(shift):
-        answer(shift).wait_recv()
+        for h in range(2):
+            answer(shift, h).wait_recv()
         mix[...] += far_in[...].astype(f32)
 
     def rows_of(p):
@@ -466,42 +519,81 @@
 
         members(g, guarded)
 
-    def choice(c):
+    def choose():
         numbers = lax.broadcasted_iota(jnp.int32, (n_sp, count), 0)
         named = [numbers == routes_ref[k : k + 1, :] for k in range(2)]
         counted = [jnp.where(mask, 1.0, 0.0).astype(bf16) for mask in named]
         earlier = jnp.where(rows_i < rows_j, 1.0, 0.0).astype(bf16)
         before = jnp.dot(counted[0] + counted[1], earlier, preferred_element_type=f32)
-        slot = jnp.sum(jnp.where(named[c], before, 0.0), axis=0, keepdims=True)
-        target = routes_ref[c : c + 1, :] * cap + slot.astype(jnp.int32)
-        slots = lax.broadcasted_iota(jnp.int32, (outgoing.shape[0], count), 0)
-        return jnp.where(slots == target, 1.0, 0.0).astype(bf16)
+        down_slots = lax.broadcasted_iota(jnp.int32, (outgoing.shape[0], count), 0).astype(f32)
+        along_slots = lax.broadcasted_iota(jnp.int32, (count, outgoing.shape[0]), 1).astype(f32)
+        chosen = jnp.zeros((outgoing.shape[0], count), f32)
+        for c in range(2):
+            slot = jnp.sum(jnp.where(named[c], before, 0.0), axis=0, keepdims=True)
+            target = (routes_ref[c : c + 1, :] * cap).astype(f32) + slot
+            chosen = chosen + jnp.where(down_slots == target, 1.0, 0.0)
+            column = jnp.broadcast_to(target, (count, count)).T[:, 0:1]
+            picks[c] = jnp.where(along_slots == column, 1.0, 0.0).astype(bf16)
+            shares[c] = jnp.broadcast_to(route_weight_ref[c : c + 1, :], (count, count)).T
+        select[...] = chosen.astype(bf16)
+
+    def square_start(k, _):
+        square_copy(k, t).start()
+        return 0
+
+    def square_wait(k, _):
+        square_copy(k, (t + k) % n_tp).wait()
+        return 0
 
     def finish_rows():
         stream = residual_ref[...].astype(f32) + mix[...].astype(bf16).astype(f32)
         stream_ref[...] = stream
         own = jnp.sum(stream * stream, axis=1, keepdims=True)
         squares[t] = jnp.broadcast_to(own, (count, count)).T[0:8, :]
-
-        def square_start(k, _):
-            square_copy(k, t).start()
-            return 0
-
-        def square_wait(k, _):
-            square_copy(k, (t + k) % n_tp).wait()
-            return 0
-
         lax.fori_loop(1, n_tp, square_start, 0)
+        rows = (stream_ref[...] * gain_ref[...]).astype(bf16)
+        outgoing[...] = jnp.dot(select[...], rows, preferred_element_type=f32).astype(bf16)
+        arrived[t, rows_of(s)] = outgoing[rows_of(s)]
+
+    def scale_copy(p, q):
+        return remote(
+            scales_out.at[rows_of(p)],
+            scales.at[rows_of(q)],
+            scale_send.at[p],
+            scale_recv.at[q],
+            "sp",
+            p,
+        )
+
+    def finish_scale():
         lax.fori_loop(1, n_tp, square_wait, 0)
         total = squares[0]
         for p in range(1, n_tp):
             total = total + squares[p]
         scale = lax.rsqrt(total[0:1, :] / (cols * n_tp) + EPS)
-        scale = jnp.broadcast_to(scale, (count, count)).T[:, 0:1]
-        normed = (stream_ref[...] * scale * gain_ref[...]).astype(bf16)
-        select = choice(0) + choice(1)
-        outgoing[...] = jnp.dot(select, normed, preferred_element_type=f32).astype(bf16)
-        arrived[t, rows_of(s)] = outgoing[rows_of(s)]
+        scale = jnp.broadcast_to(scale, (count, count)).T
+        high = scale.astype(bf16)
+        rest = scale - high.astype(f32)
+        middle = rest.astype(bf16)
+        low = (rest - middle.astype(f32)).astype(bf16)
+        terms = jnp.where(
+            rows_j == 0,
+            high.astype(f32),
+            jnp.where(
+                rows_j == 1, middle.astype(f32), jnp.where(rows_j == 2, low.astype(f32), 0.0)
+            ),
+        ).astype(bf16)
+        scales_out[...] = jnp.dot(select[...], terms, preferred_element_type=f32).astype(bf16)
+
+        def send(p, _):
+            @pl.when(p != s)
+            def _():
+                scale_copy(p, s).start()
+
+            return 0
+
+        lax.fori_loop(0, n_sp, send, 0)
+        scales[rows_of(s)] = scales_out[rows_of(s)]
 
     def dispatch_to(q):
         def body(j, _):
@@ -515,12 +607,14 @@
 
         lax.fori_loop(0, n_sp // 4, body, 0)
 
-    def dispatch_stage(i):
-        for q in range(4):
-
-            @pl.when(quarter == q)
-            def _(q=q):
-                dispatch_to(SENDS[q][i])
+    def dispatch_stage(moment):
+        for k in range(GROUPS):
+            for target, when in SENDS[k]:
+                if when == moment:
+
+                    @pl.when(eighth == k)
+                    def _(target=target):
+                        dispatch_to(target)
 
     lines = (
         [y * across + (x + k) % across for k in range(1, across)],
@@ -528,21 +622,28 @@
     )
     direct = lines[0] + lines[1]
 
-    def straight(buffer, sems, g, i, source, rows):
+    def came_from(i):
+        if i < len(lines[0]):
+            return len(lines[0]) - 1 - i
+        return len(direct) - 1 - (i - len(lines[0]))
+
+    def straight(buffer, sems, g, i, source, rows, arriving=False):
         block = buffer.at[source, rows]
-        return remote(block, block, sems[0].at[g, i], sems[1].at[g, source], "tp", direct[i])
+        there = came_from(i) if arriving else i
+        return remote(block, block, sems[0].at[g, i], sems[1].at[g, there], "tp", direct[i])
 
     def relayed(buffer, sems, g, part, i, source, target):
         block = buffer.at[source, group_rows(g, part)]
-        return remote(
-            block, block, sems[2].at[g, part, i], sems[3].at[g, source, part], "tp", target
-        )
+        over = (source % across + across - target % across) % across - 1
+        up = (source // across + down - target // across) % down - 1
+        where = up * (across - 1) + over
+        return remote(block, block, sems[2].at[g, part, i], sems[3].at[g, part, where], "tp", target)
 
     def relay(buffer, sems, g):
         for part in range(2):
             for k, source in enumerate(lines[part]):
                 i = k if part == 0 else len(lines[0]) + k
-                straight(buffer, sems, g, i, source, group_rows(g)).wait_recv()
+                straight(buffer, sems, g, i, source, group_rows(g), True).wait_recv()
                 for j, target in enumerate(lines[1 - part]):
                     relayed(
                         buffer, sems, g, part, k * len(lines[1 - part]) + j, source, target
@@ -556,14 +657,14 @@
         def _():
             source = place_of(k)
             for part in range(2):
-                relayed(buffer, sems, g, part, 0, source, source).wait_recv()
+                relayed(buffer, sems, g, part, 0, source, t).wait_recv()
 
     def finish_sends(buffer, sems, g):
         for i in range(len(direct)):
             straight(buffer, sems, g, i, t, group_rows(g)).wait_send()
         for part in range(2):
             for i in range(len(lines[0]) * len(lines[1])):
-                relayed(buffer, sems, g, part, i, t, direct[0]).wait_send()
+                relayed(buffer, sems, g, part, i, place_of(across + 1), t).wait_send()
 
     arrived_sems = (fwd_send, fwd_recv, fwd_relay_send, fwd_relay_recv)
     hidden_sems = (hid_send, hid_recv, hid_relay_send, hid_relay_recv)
@@ -595,7 +696,12 @@
 
         with jax.named_scope("units"):
             lax.fori_loop(0, n_tp, body, 0)
-        hidden[t, group_rows(g)] = (jax.nn.silu(acc_a[...]) * acc_b[...]).astype(bf16)
+        others(g, lambda p: scale_copy(p, p).wait_recv())
+        terms = scales[group_rows(g)].astype(f32)
+        scale = terms[:, 0:1] + (terms[:, 1:2] + terms[:, 2:3])
+        hidden[t, group_rows(g)] = (
+            jax.nn.silu(acc_a[...] * scale) * (acc_b[...] * scale)
+        ).astype(bf16)
         for i in range(len(direct)):
             straight(hidden, hidden_sems, g, i, t, group_rows(g)).start()
 
@@ -629,87 +735,145 @@
         with jax.named_scope("relay_hidden"):
             relay(hidden, hidden_sems, g)
 
+    mix[...] = jnp.zeros_like(mix)
+    choose()
+    with jax.named_scope("right"):
+        serve_right(1)
     with jax.named_scope("proj1"):
-        project_chips(1, True)
-    with jax.named_scope("proj2"):
-        lax.fori_loop(2, reach + 1, project_far, 0)
-    far_pair(near_low, -2, project_edge)
-    far_pair(near_high, 2, project_edge)
+        for h in range(2):
+            for i in range(2):
+                project(z * 2 + i, h)
+            project_chips(1, h)
+
+    def project_far(j, _):
+        for h in range(2):
+            if h == 0:
+                for i in range(2):
+                    serve(j, 0, i)
+            else:
+                serve_right(j)
+            project_chips(j, h)
+        return 0
+
+    lax.fori_loop(2, reach, project_far, 0)
+    far_pair(near_low, -2, lambda shift: ask(shift).wait_recv())
+    far_pair(near_high, 2, lambda shift: ask(shift).wait_recv())
+    for h in range(2):
+        with jax.named_scope("far"):
+            for i in range(2):
+                serve(reach, h, i)
+            project_chips(reach, h)
+        far_pair(near_low, -2, lambda shift, h=h: project_edge(shift, h))
+        far_pair(near_high, 2, lambda shift, h=h: project_edge(shift, h))
     with jax.named_scope("edge"):
         far_pair(at_low, 2, add_edge)
         far_pair(at_high, -2, add_edge)
     with jax.named_scope("finish"):
         finish_rows()
-    dispatch_stage(0)
     dispatch_to(quarter)
+    dispatch_stage(-2)
+    forward(0)
+    with jax.named_scope("scale"):
+        finish_scale()
     for load in loads:
         load.wait()
-    for step in range(GROUPS + 4):
-        for late, action in enumerate(
-            (forward, relay_rows, through_units, relay_hidden, through_down)
-        ):
-            if 0 <= step - late < GROUPS:
-                action(step - late)
-            if late == 1 and step in (1, 3):
-                dispatch_stage((step + 1) // 2)
+    dispatch_stage(-1)
+
+    def early_sends():
+        @pl.when(s < n_sp - 1)
+        def _():
+            def gone(c, _):
+                hop(c).wait_send()
+                return 0
+
+            lax.fori_loop(0, total_pieces, gone, 0)
+
+        for g in range(2):
+
+            def heads_gone(k, _, g=g):
+                heads_copy(g, k, t).wait_send()
+                return 0
+
+            lax.fori_loop(1, n_tp, heads_gone, 0)
+
+        def passed(j, _):
+            chip = chip_behind(j)
+
+            @pl.when((chip >= 0) & (chip < chips))
+            def _():
+                for i in range(2):
+                    b = chip * 2 + i
+
+                    @pl.when(has_ahead & (j < reach))
+                    def _():
+                        @pl.when(j == 0)
+                        def _():
+                            along_line(b, 0).wait_send()
+
+                        along_line(b, 1).wait_send()
+
+                    @pl.when((b == s) | (j > 0))
+                    def _():
+                        for h in range(2):
+                            to_partner(b, h).wait_send()
+
+            return 0
+
+        lax.fori_loop(0, reach + 1, passed, 0)
+        far_pair(at_low, 2, lambda shift: ask(shift).wait_send())
+        far_pair(at_high, -2, lambda shift: ask(shift).wait_send())
+        for h in range(2):
+            far_pair(near_low, -2, lambda shift, h=h: answer(shift, h).wait_send())
+            far_pair(near_high, 2, lambda shift, h=h: answer(shift, h).wait_send())
+
+    for step in range(GROUPS):
+        if step > 0:
+            dispatch_stage(step)
+            forward(step)
+            relay_rows(step - 1)
+        if step >= 2:
+            through_units(step - 2)
+        if step >= 3:
+            relay_hidden(step - 3)
+        if step == 3:
+            early_sends()
+        if step >= 4:
+            through_down(step - 4)
+            finish_sends(arrived, arrived_sems, step - 4)
+    last = GROUPS - 1
+    relay_rows(last)
+    through_units(last - 1)
+    relay_hidden(last - 2)
+    through_units(last)
+    relay_hidden(last - 1)
+    for g in range(last - 3, last - 1):
+        through_down(g)
+    relay_hidden(last)
+    for g in range(last - 1, last + 1):
+        through_down(g)
+    for g in range(GROUPS):
+        others(g, lambda p: dispatch(p, s).wait_send())
+        others(g, lambda p: scale_copy(p, s).wait_send())
+        if g >= last - 3:
+            finish_sends(arrived, arrived_sems, g)
+        finish_sends(hidden, hidden_sems, g)
 
     returned[rows_of(s)] = result[rows_of(s)]
     with jax.named_scope("back"):
         for g in range(GROUPS):
             others(g, lambda p: give_back(p, p).wait_recv())
+    combine_scope = jax.named_scope("combine")
+    combine_scope.__enter__()
     total = stream_ref[...]
     for c in range(2):
-        pick = lax.dot_general(
-            choice(c), returned[...], (((0,), (0,)), ((), ())), preferred_element_type=f32
-        )
-        share = jnp.broadcast_to(route_weight_ref[c : c + 1, :], (count, count)).T[:, 0:1]
-        total = total + share * pick
+        pick = jnp.dot(picks[c], returned[...], preferred_element_type=f32)
+        total = total + shares[c][:, 0:1] * pick
     out_ref[...] = total.astype(bf16)
-
-    @pl.when(s < n_sp - 1)
-    def _():
-        def gone(c, _):
-            hop(c).wait_send()
-            return 0
-
-        lax.fori_loop(0, total_pieces, gone, 0)
-
-    for g in range(2):
-
-        def heads_gone(k, _, g=g):
-            heads_copy(g, k, t).wait_send()
-            return 0
-
-        lax.fori_loop(1, n_tp, heads_gone, 0)
-
-    def passed(j, _):
-        chip = chip_behind(j)
-
-        @pl.when((chip >= 0) & (chip < chips))
-        def _():
-            for i in range(2):
-                b = chip * 2 + i
-
-                @pl.when(has_ahead & (j < reach))
-                def _():
-                    along_line(b).wait_send()
-
-                @pl.when((b == s) | (j > 0))
-                def _():
-                    to_partner(b).wait_send()
-
-        return 0
-
-    lax.fori_loop(0, reach + 1, passed, 0)
-    far_pair(at_low, 2, lambda shift: ask(shift).wait_send())
-    far_pair(at_high, -2, lambda shift: ask(shift).wait_send())
-    far_pair(near_low, -2, lambda shift: answer(shift).wait_send())
-    far_pair(near_high, 2, lambda shift: answer(shift).wait_send())
-    for g in range(GROUPS):
-        others(g, lambda p: dispatch(p, s).wait_send())
-        others(g, lambda p: give_back(p, s).wait_send())
-        finish_sends(arrived, arrived_sems, g)
-        finish_sends(hidden, hidden_sems, g)
+    combine_scope.__exit__(None, None, None)
+
+    with jax.named_scope("sent"):
+        for g in range(GROUPS):
+            others(g, lambda p: give_back(p, s).wait_send())
 
 
 def tables(rows, blocks, size):
@@ -759,12 +923,35 @@
     straights, relays = across + down - 2, (across - 1) * (down - 1)
     vmem = pl.BlockSpec(memory_space=pltpu.VMEM)
     hbm = pl.BlockSpec(memory_space=pl.ANY)
+    inputs = (
+        residual,
+        query_small,
+        key_narrow_group,
+        query_large,
+        key_large,
+        values,
+        gates,
+        turn_a,
+        start_a,
+        turn_b,
+        start_b,
+        jnp.transpose(log_decay, (1, 2, 0)).reshape(2 * head_count, row_count),
+        head_gain,
+        norm_gain[None, :],
+        routes.T,
+        route_weight.T,
+    )
     return pl.pallas_call(
         layer_kernel,
         out_shape=jax.ShapeDtypeStruct((row_count, cols), bf16),
-        in_specs=[vmem] * 16 + [hbm] * 4,
+        in_specs=[hbm] * (STAGED + 4),
         out_specs=vmem,
-        scratch_shapes=[
+        scratch_shapes=[pltpu.VMEM(a.shape, a.dtype) for a in inputs]
+        + [
+            dma((STAGED,)),
+            pltpu.VMEM((2, row_count, slots), bf16),
+            pltpu.VMEM((slots, row_count), bf16),
+            pltpu.VMEM((2, row_count, row_count), f32),
             pltpu.VMEM((row_count, cols), f32),
             pltpu.VMEM((row_count, 2 * head_count), f32),
             pltpu.VMEM((2 * head_count, row_count), f32),
@@ -785,6 +972,8 @@
             pltpu.VMEM((slots, cols), bf16),
             pltpu.VMEM((n_tp, slots, cols), bf16),
             pltpu.VMEM((n_tp, slots, units), bf16),
+            pltpu.VMEM((slots, 128), bf16),
+            pltpu.VMEM((slots, 128), bf16),
             pltpu.VMEM((2, row_count, values.shape[2]), bf16),
             pltpu.VMEM((row_count, cols), bf16),
             pltpu.VMEM((row_count, cols), bf16),
@@ -798,51 +987,32 @@
             dma((pieces,)),
             dma((2, n_tp)),
             dma((2, n_tp)),
-            dma((n_sp,)),
-            dma((n_sp,)),
-            dma((n_sp,)),
-            dma((2,)),
-            dma((2,)),
+            dma((2, n_sp)),
+            dma((2, n_sp)),
+            dma((2, n_sp)),
+            dma((3,)),
+            dma((3,)),
             dma((n_tp,)),
             dma((n_tp,)),
             dma((n_sp,)),
             dma((n_sp,)),
+            dma((n_sp,)),
+            dma((n_sp,)),
             dma((GROUPS, straights)),
-            dma((GROUPS, n_tp)),
+            dma((GROUPS, straights)),
             dma((GROUPS, 2, relays)),
-            dma((GROUPS, n_tp, 2)),
+            dma((GROUPS, 2, relays)),
             dma((GROUPS, straights)),
-            dma((GROUPS, n_tp)),
+            dma((GROUPS, straights)),
             dma((GROUPS, 2, relays)),
-            dma((GROUPS, n_tp, 2)),
+            dma((GROUPS, 2, relays)),
             dma((n_sp,)),
             dma((n_sp,)),
         ],
         compiler_params=pltpu.CompilerParams(
             collective_id=0, has_side_effects=True, vmem_limit_bytes=58 * 2**20
         ),
-    )(
-        residual,
-        query_small,
-        key_narrow_group,
-        query_large,
-        key_large,
-        values,
-        gates,
-        turn_a,
-        start_a,
-        turn_b,
-        start_b,
-        jnp.transpose(log_decay, (1, 2, 0)).reshape(2 * head_count, row_count),
-        head_gain,
-        norm_gain[None, :],
-        routes.T,
-        route_weight.T,
-        out_weight,
-        expert_gate,
-        expert_up,
-        expert_down,
-    )
+    )(*inputs, out_weight, expert_gate, expert_up, expert_down)
 
 
 def solution(mesh):

time: 136 us -> 133 us (0.978)
  Pallas kernels: 133 us -> 131 us
    pallas_call x1, Pallas kernels: 133 us -> 131 us  [per_device(): pl.pallas_call(layer_kernel, out_shape=jax.ShapeDtypeStruct((row_count, c...]
where the time goes in v4:
time: 133 us
  Pallas kernels  131 us (98%)
  local copies, waits for them, and re-layouts  1.67 us (1%)
    pallas_call x1, Pallas kernels, per_device(): pl.pallas_call(layer_kernel, out_shape=jax.ShapeDtypeStruct((row_count, c...  131 us

profile of v4, /device:TPU:1, one launch (start us, length us, event | category | flops | bytes accessed | tf_op | source)
XLA Modules:
  0.0 132.8 jit_solution(12172012082645154283)
XLA Ops:
  0.0 131.1 %shard_map.190 = bf16[128,1024]{1,0:T(8,128)(2,1)} custom-call(bf16[128,1024]{1,0:T(8,128)(2,1)} %refs_0_.1, bf16[128,512]{1,0:T(8,128)(2,1)} %refs_1_.1, bf16[128,512]{1,0:T(8,128)(2,1)} %refs_2_.1, bf16[128,1024]{1,0:T(8,128)(2,1)} %refs_3_.1, bf16[128,1024]{1,0:T(8,128)(2,1)} %refs_4_.1, bf16[128,2,512]{2,1,0:T(2,128)(2,1)} %refs_5_.1, ...), custom_call_target="tpu_custom_call" | custom-call | tf_op jit(solution)/shard_map/pallas_call | solution.py:944
  131.1 1.7 %copy.22 = bf16[128,1024]{1,0:T(8,128)(2,1)} copy(bf16[128,1024]{1,0:T(8,128)(2,1)} %shard_map.190) | data formatting | bytes 524288

commit v5 on v4

--- a/solution.py
+++ b/solution.py
@@ -843,14 +843,14 @@
     last = GROUPS - 1
     relay_rows(last)
     through_units(last - 1)
+    through_down(last - 3)
     relay_hidden(last - 2)
     through_units(last)
+    through_down(last - 2)
     relay_hidden(last - 1)
-    for g in range(last - 3, last - 1):
-        through_down(g)
+    through_down(last - 1)
     relay_hidden(last)
-    for g in range(last - 1, last + 1):
-        through_down(g)
+    through_down(last)
     for g in range(GROUPS):
         others(g, lambda p: dispatch(p, s).wait_send())
         others(g, lambda p: scale_copy(p, s).wait_send())

time: 133 us -> 132 us (level)
  no operation moved by 1% of the time
where the time goes in v5:
time: 132 us
  Pallas kernels  131 us (99%)
  local copies, waits for them, and re-layouts  1.67 us (1%)
    pallas_call x1, Pallas kernels, per_device(): pl.pallas_call(layer_kernel, out_shape=jax.ShapeDtypeStruct((row_count, c...  131 us

profile of v5, /device:TPU:1, one launch (start us, length us, event | category | flops | bytes accessed | tf_op | source)
XLA Modules:
  0.0 132.3 jit_solution(397171433987385064)
XLA Ops:
  0.0 130.7 %shard_map.190 = bf16[128,1024]{1,0:T(8,128)(2,1)} custom-call(bf16[128,1024]{1,0:T(8,128)(2,1)} %refs_0_.1, bf16[128,512]{1,0:T(8,128)(2,1)} %refs_1_.1, bf16[128,512]{1,0:T(8,128)(2,1)} %refs_2_.1, bf16[128,1024]{1,0:T(8,128)(2,1)} %refs_3_.1, bf16[128,1024]{1,0:T(8,128)(2,1)} %refs_4_.1, bf16[128,2,512]{2,1,0:T(2,128)(2,1)} %refs_5_.1, ...), custom_call_target="tpu_custom_call" | custom-call | tf_op jit(solution)/shard_map/pallas_call | solution.py:944
  130.7 1.7 %copy.22 = bf16[128,1024]{1,0:T(8,128)(2,1)} copy(bf16[128,1024]{1,0:T(8,128)(2,1)} %shard_map.190) | data formatting | bytes 524288
